TPU v7x, 256 devices: a 8x8x2 block of a 8x8x16 slice. The times are simulated.
256 devices in a mesh: grp: 2 (over z), ep: 64 (over y, x), tp: 2 (over core).
Axes of the slice: x: 8, y: 8, z: 2, core: 2. Of those that a mesh axis runs over, the one named last changes fastest.
The devices are a block of a 8x8x16 slice.
Arguments:
- hidden_in: bfloat16 [2048, 2048], P(('grp', 'ep', 'tp')), parts along dimension 0, may hold values from -6 to 6
- query_nope: bfloat16 [2048, 16, 64], P(('grp', 'ep', 'tp')), parts along dimension 0, may hold values from -102 to 102
- query_rope: bfloat16 [2048, 16, 32], P(('grp', 'ep', 'tp')), parts along dimension 0, may hold values from -6 to 6
- new_latent: bfloat16 [2048, 256], P(('grp', 'ep', 'tp')), parts along dimension 0, may hold values from -6 to 6
- new_rope: bfloat16 [2048, 32], P(('grp', 'ep', 'tp')), parts along dimension 0, may hold values from -6 to 6
- cache_latent: bfloat16 [2048, 1024, 256], P(('grp', 'ep', 'tp')), parts along dimension 0, may hold values from -6 to 6
- cache_rope: bfloat16 [2048, 1024, 32], P(('grp', 'ep', 'tp')), parts along dimension 0, may hold values from -6 to 6
- lengths: int32 [2048], P(('grp', 'ep', 'tp')), parts along dimension 0, may hold values from 1 to 1024, as said below
- absorb_key: bfloat16 [256, 16, 64], replicated, may hold values from -0.75 to 0.75
- value_up: bfloat16 [256, 16, 128], replicated, may hold values from -0.375 to 0.375
- out_proj: bfloat16 [2048, 2048], P(None, ('ep', 'tp')), may hold values from -0.125 to 0.125
- gain_mix: bfloat16 [2048], replicated, may hold values from 0.099609375 to 1.8984375
- gain_ffn_in: bfloat16 [2048], replicated, may hold values from 0.099609375 to 1.8984375
- router: bfloat16 [2048, 128], replicated, may hold values from -0.125 to 0.125
- routes: int32 [2048, 6], P(('grp', 'ep')), parts along dimension 0, may hold values from 0 to 127, all different within a row; in each aligned block of 16 rows (0 to 15, 16 to 31, ...) at most 2 rows name the same one
- expert_gate: bfloat16 [128, 2048, 256], P(('ep', 'tp')), may hold values from -0.125 to 0.125
- expert_up: bfloat16 [128, 2048, 256], P(('ep', 'tp')), may hold values from -0.125 to 0.125
- expert_down: bfloat16 [128, 256, 2048], P(('ep', 'tp')), may hold values from -0.375 to 0.375
- shared_gate: bfloat16 [2048, 256], replicated, may hold values from -0.125 to 0.125
- shared_up: bfloat16 [2048, 256], replicated, may hold values from -0.125 to 0.125
- shared_down: bfloat16 [256, 2048], replicated, may hold values from -0.375 to 0.375
- gain_ffn_out: bfloat16 [2048], replicated, may hold values from 0.099609375 to 1.8984375
Outputs:
- layer_out: bfloat16 [2048, 2048], P(('grp', 'ep', 'tp')), parts along dimension 0
There are 2 independent parts, one for each index of `grp`. A program takes and returns all parts, laid end to end along the dimension named above; an argument that names none is the same for every part. Nothing has to cross between parts.
Inputs may be any that keep to these rules, and one draw needn't show every extreme that they name: `lengths`: every sequence holds 1 to 1024 cached positions, and some sequence holds 1024. `routes`: each row names 6 different experts; in each aligned block of 16 rows (the rows of one index of ep) no expert is named by more than 2 rows, and in some block some expert is named by exactly 2 rows.
All inputs are finite; a program needn't handle non-finite values.
Results may differ from a plain program's by a relative error of at most 0.015.
Values may be sent and summed in bfloat16 or wider, within the bound.
No kernel may reach another device: no remote copies, remote signals or barrier semaphores. Data moves between devices by JAX's collectives and lax.ppermute only.
A program may use at most 64 MiB of HBM per device.

v0:
```python
import jax
import jax.numpy as jnp
from jax import lax
from jax.experimental import pallas as pl
from jax.experimental.pallas import tpu as pltpu
from jax.sharding import Mesh
from jax.sharding import PartitionSpec as P

SEQ_STEP = 2
EP = ("ep_0", "ep_1")
GRP_EP_TP = ("grp", "ep_0", "ep_1", "tp")
EP_TP = ("ep_0", "ep_1", "tp")
GRP_EP = ("grp", "ep_0", "ep_1")


rope_theta = 10000.0
norm_eps = 1e-06
routed_scale = 2.5
masked_score = -1e30


def device_at(row, col, core):
    return (row * 8 + col) * 2 + core


PLACES = [
    [
        device_at(2 * block_row + i, 2 * block_col + j, core)
        for block_row in range(4)
        for block_col in range(4)
    ]
    for i in range(2)
    for j in range(2)
    for core in range(2)
]


def partners(flip_i, flip_j):
    return [
        (device_at(row, col, core), device_at(row ^ flip_i, col ^ flip_j, core))
        for row in range(8)
        for col in range(8)
        for core in range(2)
    ]


def from_partner(array, flip):
    return lax.ppermute(array, EP_TP, partners(flip // 2, flip % 2))


def exchanged(blocks, groups):
    return lax.all_to_all(blocks, EP_TP, 0, 0, axis_index_groups=groups, tiled=True)


def sent_to_all(array, groups):
    count = len(groups[0])
    return exchanged(jnp.broadcast_to(array[None], (count, *array.shape)), groups)


def from_other_core(array):
    return lax.ppermute(array, "tp", [(0, 1), (1, 0)])


def normalize(values):
    return values * lax.rsqrt(jnp.mean(values * values, axis=-1, keepdims=True) + norm_eps)


def swiglu(flat_rows, gate_w, up_w, down_w):
    gate_part = jnp.dot(flat_rows, gate_w, preferred_element_type=jnp.float32)
    up_part = jnp.dot(flat_rows, up_w, preferred_element_type=jnp.float32)
    inner_rows = (jax.nn.silu(gate_part) * up_part).astype(jnp.bfloat16)
    return jnp.dot(inner_rows, down_w, preferred_element_type=jnp.float32).astype(jnp.bfloat16)


def attention_kernel(
    lengths_ref,
    nope_ref,
    rope_ref,
    latent_ref,
    key_ref,
    cosine_ref,
    sine_ref,
    absorb_ref,
    cache_ref,
    cache_rope_ref,
    out_ref,
    query_ref,
    query_pe_ref,
    latent_new_ref,
    key_new_ref,
):
    step = pl.program_id(0)
    seq_count, heads, nope = nope_ref.shape
    rope = rope_ref.shape[-1]
    half = rope // 2
    latent = cache_ref.shape[-1]
    scale = (nope + rope) ** (-0.5)

    def turned(values, cosine, sine):
        swapped = jnp.concatenate([values[..., half:], values[..., :half]], axis=-1)
        return values * cosine + swapped * sine

    @pl.when(step == 0)
    def _():
        rows = nope_ref[...].reshape(seq_count * heads, nope)
        twice = jnp.concatenate([rows, rows], axis=-1)
        wide = jnp.concatenate([twice] * (heads // 2), axis=-1)
        row_head = lax.broadcasted_iota(jnp.int32, wide.shape, 0) % heads
        column_head = lax.broadcasted_iota(jnp.int32, wide.shape, 1) // nope
        wide = jnp.where(row_head == column_head, wide.astype(jnp.float32), 0.0)
        queries = jnp.dot(
            wide.astype(jnp.bfloat16), absorb_ref[...], preferred_element_type=jnp.float32
        )
        query_ref[...] = queries.reshape(seq_count, heads, latent).astype(jnp.bfloat16)
        cosine = cosine_ref[...][:, None, :]
        sine = sine_ref[...][:, None, :]
        query_pe_ref[...] = turned(rope_ref[...].astype(jnp.float32), cosine, sine).astype(
            jnp.bfloat16
        )
        latent_new = normalize(latent_ref[...].astype(jnp.float32)).astype(jnp.bfloat16)
        latent_new_ref[...] = latent_new.astype(jnp.float32)[:, None, :]
        key_new = turned(key_ref[...].astype(jnp.float32), cosine_ref[...], sine_ref[...])
        key_new_ref[...] = key_new.astype(jnp.bfloat16).astype(jnp.float32)[:, None, :]

    for place in range(cache_ref.shape[0]):
        seq = step * cache_ref.shape[0] + place
        length = lengths_ref[seq]
        query = query_ref[seq]
        query_pe = query_pe_ref[seq]
        latent_wide = latent_new_ref[seq]
        score_new = (
            jnp.sum(query.astype(jnp.float32) * latent_wide, axis=-1, keepdims=True)
            + jnp.sum(query_pe.astype(jnp.float32) * key_new_ref[seq], axis=-1, keepdims=True)
        ) * scale
        cache = cache_ref[place]
        scores = (
            lax.dot_general(
                query, cache, (((1,), (1,)), ((), ())), preferred_element_type=jnp.float32
            )
            + jnp.dot(query_pe, cache_rope_ref[place], preferred_element_type=jnp.float32)
        ) * scale
        position = lax.broadcasted_iota(jnp.int32, scores.shape, 1)
        scores = jnp.where(position < length, scores, masked_score)
        row_max = jnp.maximum(jnp.max(scores, axis=-1, keepdims=True), score_new)
        weights = jnp.exp(scores - row_max)
        weight_new = jnp.exp(score_new - row_max)
        total = jnp.sum(weights, axis=-1, keepdims=True) + weight_new
        summed = (
            jnp.dot(weights.astype(jnp.bfloat16), cache, preferred_element_type=jnp.float32)
            + weight_new.astype(jnp.bfloat16).astype(jnp.float32) * latent_wide
        )
        out_ref[place] = (summed / total).astype(jnp.bfloat16)


def attended(query_nope, query_rope, new_latent, new_rope, cache_latent, cache_rope, lengths, absorb_key):
    seq_count, heads, nope = query_nope.shape
    rope = query_rope.shape[-1]
    latent = cache_latent.shape[-1]
    context = cache_latent.shape[1]
    half = rope // 2
    inverse = rope_theta ** (-jnp.arange(half, dtype=jnp.float32) * 2.0 / rope)
    angles = lengths.astype(jnp.float32)[:, None] * jnp.concatenate([inverse, inverse])[None, :]
    sign = jnp.where(jnp.arange(rope) < half, -1.0, 1.0)
    cosine = jnp.cos(angles)
    sine = jnp.sin(angles) * sign[None, :]
    absorb = absorb_key.transpose(1, 2, 0).reshape(heads * nope, latent)
    rope_turned = cache_rope.transpose(0, 2, 1)
    whole = lambda *shape: pl.BlockSpec(shape, lambda step, lengths: (0,) * len(shape))
    return pl.pallas_call(
        attention_kernel,
        grid_spec=pltpu.PrefetchScalarGridSpec(
            num_scalar_prefetch=1,
            grid=(seq_count // SEQ_STEP,),
            in_specs=[
                whole(seq_count, heads, nope),
                whole(seq_count, heads, rope),
                whole(seq_count, latent),
                whole(seq_count, rope),
                whole(seq_count, rope),
                whole(seq_count, rope),
                whole(heads * nope, latent),
                pl.BlockSpec((SEQ_STEP, context, latent), lambda step, lengths: (step, 0, 0)),
                pl.BlockSpec((SEQ_STEP, rope, context), lambda step, lengths: (step, 0, 0)),
            ],
            out_specs=pl.BlockSpec((SEQ_STEP, heads, latent), lambda step, lengths: (step, 0, 0)),
            scratch_shapes=[
                pltpu.VMEM((seq_count, heads, latent), jnp.bfloat16),
                pltpu.VMEM((seq_count, heads, rope), jnp.bfloat16),
                pltpu.VMEM((seq_count, 1, latent), jnp.float32),
                pltpu.VMEM((seq_count, 1, rope), jnp.float32),
            ],
        ),
        out_shape=jax.ShapeDtypeStruct((seq_count, heads, latent), jnp.bfloat16),
        compiler_params=pltpu.CompilerParams(dimension_semantics=("arbitrary",)),
        cost_estimate=pl.CostEstimate(
            flops=8 * seq_count * heads * context * latent,
            bytes_accessed=2 * seq_count * context * (latent + rope),
            transcendentals=seq_count * heads * context,
        ),
        name="attended",
    )(
        lengths, query_nope, query_rope, new_latent, new_rope, cosine, sine, absorb, cache_latent, rope_turned
    )


def attention(
    query_nope,
    query_rope,
    new_latent,
    new_rope,
    cache_latent,
    cache_rope,
    lengths,
    absorb_key,
    value_up,
):
    latent_out = attended(
        query_nope, query_rope, new_latent, new_rope, cache_latent, cache_rope, lengths, absorb_key
    )
    return (
        jnp.einsum("shc,chv->shv", latent_out, value_up, preferred_element_type=jnp.float32)
        .astype(jnp.bfloat16)
        .reshape(latent_out.shape[0], -1)
    )


def spread_kernel(
    place_ref,
    pieces_ref,
    hidden_ref,
    gain_mix_ref,
    gain_in_ref,
    routes_ref,
    outgoing_ref,
    ffn_ref,
    mix_ref,
    taken_ref,
):
    core, block_i, block_j = place_ref[0], place_ref[1], place_ref[2]
    rows, _ = hidden_ref.shape
    piece = pieces_ref.shape[-1]
    run = piece // 4
    chunks = []
    for block_row in range(4):
        for i in range(2):
            runs = [
                pieces_ref[
                    c,
                    (i ^ block_i) * 2 + (j ^ block_j),
                    :,
                    block_row * run : (block_row + 1) * run,
                ]
                for j in range(2)
                for c in range(2)
            ]
            chunks.append(jnp.concatenate(runs, axis=-1))
    joined = jnp.concatenate(chunks, axis=0)
    source = lax.broadcasted_iota(jnp.int32, (piece, piece), 0)
    target = lax.broadcasted_iota(jnp.int32, (piece, piece), 1)
    k = run // 4
    goes_to = (source % run) // k * run + source // run * k + source % k
    order = jnp.where(goes_to == target, 1.0, 0.0).astype(jnp.bfloat16)
    placed = jnp.dot(joined, order, preferred_element_type=jnp.float32)
    mixed = jnp.concatenate(
        [placed[n * rows : (n + 1) * rows] for n in range(len(chunks))], axis=-1
    )
    after_mix = (
        hidden_ref[...].astype(jnp.float32)
        + gain_mix_ref[...].astype(jnp.float32) * normalize(mixed)
    ).astype(jnp.bfloat16)
    after_wide = after_mix.astype(jnp.float32)
    ffn_in = (normalize(after_wide) * gain_in_ref[...].astype(jnp.float32)).astype(jnp.bfloat16)
    ffn_ref[...] = ffn_in
    half = rows // 2
    mix_ref[...] = jnp.where(core == 0, after_wide[:half], after_wide[half:]).astype(jnp.bfloat16)
    slots = outgoing_ref.shape[0]
    slot = lax.broadcasted_iota(jnp.int32, (rows, slots), 1)
    expert = slot // 2 * 2 + core
    named = jnp.zeros((rows, slots), jnp.float32)
    for n in range(routes_ref.shape[1]):
        named = jnp.where(routes_ref[:, n : n + 1] == expert, 1.0, named)
    earlier = jnp.where(
        lax.broadcasted_iota(jnp.int32, (rows, rows), 1)
        < lax.broadcasted_iota(jnp.int32, (rows, rows), 0),
        1.0,
        0.0,
    ).astype(jnp.bfloat16)
    before = jnp.dot(earlier, named.astype(jnp.bfloat16), preferred_element_type=jnp.float32)
    taken = jnp.where(before == (slot % 2).astype(jnp.float32), named, 0.0).astype(jnp.bfloat16)
    taken_ref[...] = taken
    outgoing_ref[...] = lax.dot_general(
        taken, ffn_in, (((0,), (0,)), ((), ())), preferred_element_type=jnp.float32
    ).astype(jnp.bfloat16)


def spread(place, pieces, chip_hidden, gain_mix, gain_in, routes, slots):
    rows, width = chip_hidden.shape
    return pl.pallas_call(
        spread_kernel,
        in_specs=[pl.BlockSpec(memory_space=pltpu.SMEM)]
        + [pl.BlockSpec(memory_space=pltpu.VMEM)] * 5,
        out_specs=[pl.BlockSpec(memory_space=pltpu.VMEM)] * 4,
        out_shape=[
            jax.ShapeDtypeStruct((slots, width), jnp.bfloat16),
            jax.ShapeDtypeStruct((rows, width), jnp.bfloat16),
            jax.ShapeDtypeStruct((rows // 2, width), jnp.bfloat16),
            jax.ShapeDtypeStruct((rows, slots), jnp.bfloat16),
        ],
        name="spread",
    )(place, pieces, chip_hidden, gain_mix[None], gain_in[None], routes)


def local(
    hidden_in,
    query_nope,
    query_rope,
    new_latent,
    new_rope,
    cache_latent,
    cache_rope,
    lengths,
    absorb_key,
    value_up,
    out_proj,
    gain_mix,
    gain_ffn_in,
    router,
    routes,
    expert_gate,
    expert_up,
    expert_down,
    shared_gate,
    shared_up,
    shared_down,
    gain_ffn_out,
):
    seq_count, width = hidden_in.shape
    core = lax.axis_index("tp")
    own_start = core * seq_count
    slab = sent_to_all(out_proj.T, PLACES).reshape(-1, out_proj.shape[0])
    chip_hidden = lax.all_gather(hidden_in, "tp", axis=0, tiled=True)
    heads_out = attention(
        query_nope,
        query_rope,
        new_latent,
        new_rope,
        cache_latent,
        cache_rope,
        lengths,
        absorb_key,
        value_up,
    )
    chip_heads = lax.all_gather(heads_out, "tp", axis=0, tiled=True)
    block_heads = jnp.concatenate(
        [chip_heads] + [from_partner(chip_heads, flip) for flip in range(1, 4)], axis=0
    )
    partial = lax.dot_general(
        block_heads, slab, (((1,), (1,)), ((), ())), preferred_element_type=jnp.float32
    ).astype(jnp.bfloat16)
    chip_rows = partial.reshape(4, 2 * seq_count, -1)
    pieces = jnp.stack(
        [chip_rows[0]] + [from_partner(chip_rows[flip], flip) for flip in range(1, 4)]
    )
    pieces = lax.all_gather(pieces, "tp", axis=0)
    place = jnp.stack([core, lax.axis_index("ep_0") % 2, lax.axis_index("ep_1") % 2])
    experts_total = router.shape[1]
    group_rows, top_count = routes.shape
    ep_count = lax.axis_size(EP)
    capacity = 2 * ((group_rows * top_count + experts_total - 1) // experts_total)
    slots = ep_count * capacity
    slot_expert = lax.iota(jnp.int32, slots) // capacity * 2 + core
    outgoing, ffn_in, own_mix, taken = spread(
        place.astype(jnp.int32), pieces, chip_hidden, gain_mix, gain_ffn_in, routes, slots
    )
    received = lax.all_to_all(
        outgoing.reshape(ep_count, capacity, width), EP, split_axis=0, concat_axis=0, tiled=True
    )
    affinity = jax.nn.sigmoid(jnp.dot(ffn_in, router, preferred_element_type=jnp.float32))
    choose = routes[..., None] == lax.iota(jnp.int32, experts_total)[None, None, :]
    chosen = jnp.sum(jnp.where(choose, affinity[:, None, :], 0.0), axis=-1)
    route_weights = chosen / jnp.sum(chosen, axis=-1, keepdims=True) * routed_scale
    slot_weights = jnp.sum(
        jnp.where(
            routes[:, :, None] == slot_expert[None, None, :], route_weights[:, :, None], 0.0
        ),
        axis=1,
    )
    slot_weights = slot_weights * taken.astype(jnp.float32)
    weights_high = slot_weights.astype(jnp.bfloat16)
    weights_low = (slot_weights - weights_high.astype(jnp.float32)).astype(jnp.bfloat16)
    own_ffn = lax.dynamic_slice_in_dim(ffn_in, own_start, seq_count, 0)
    shared = swiglu(own_ffn, shared_gate, shared_up, shared_down)
    outputs = swiglu(
        received.reshape(slots, width), expert_gate[0], expert_up[0], expert_down[0]
    )
    returned = lax.all_to_all(
        outputs.reshape(ep_count, capacity, width), EP, split_axis=0, concat_axis=0, tiled=True
    ).reshape(slots, width)
    both = jnp.dot(
        jnp.concatenate([weights_high, weights_low], axis=0),
        returned,
        preferred_element_type=jnp.float32,
    )
    routed = both[:group_rows] + both[group_rows:]
    kept = lax.dynamic_slice_in_dim(routed, own_start, seq_count, 0)
    given = lax.dynamic_slice_in_dim(routed, seq_count - own_start, seq_count, 0)
    combined = kept + from_other_core(given) + shared.astype(jnp.float32)
    return (
        own_mix.astype(jnp.float32) + gain_ffn_out.astype(jnp.float32) * normalize(combined)
    ).astype(jnp.bfloat16)


def solution(mesh):
    torus = Mesh(
        mesh.devices.reshape(mesh.shape["grp"], 8, 8, mesh.shape["tp"]),
        ("grp", "ep_0", "ep_1", "tp"),
    )
    in_specs = (
        P(GRP_EP_TP, None),
        P(GRP_EP_TP, None, None),
        P(GRP_EP_TP, None, None),
        P(GRP_EP_TP, None),
        P(GRP_EP_TP, None),
        P(GRP_EP_TP, None, None),
        P(GRP_EP_TP, None, None),
        P(GRP_EP_TP),
        P(),
        P(),
        P(None, EP_TP),
        P(),
        P(),
        P(),
        P(GRP_EP, None),
        P(EP_TP, None, None),
        P(EP_TP, None, None),
        P(EP_TP, None, None),
        P(),
        P(),
        P(),
        P(),
    )
    out_specs = P(GRP_EP_TP, None)

    return jax.shard_map(local, mesh=torus, in_specs=in_specs, out_specs=out_specs, check_vma=False)
```

profile of v0, /device:TPU:513, one launch (start us, length us, event | category | flops | bytes accessed | tf_op | source)
XLA Modules:
  0.0 133.0 jit_solution(10931935014800736659)
XLA Ops:
  0.0 0.0 copy-start
  0.0 0.0 copy-start.3
  0.0 2.1 %broadcast_in_dim.56 = bf16[16,16,2048]{2,1,0:T(8,128)(2,1)} broadcast(bf16[16,2048]{1,0:T(8,128)(2,1)} %bitcast.41), dimensions={1,2} | broadcast | bytes 1114112 | tf_op jit(solution)/shard_map/broadcast_in_dim | solution.py:57
  2.1 19.1 %all-to-all-start = ((bf16[16,16,2048]{2,1,0:T(8,128)(2,1)}), bf16[16,16,2048]{2,1,0:T(8,128)(2,1)}, u32[]{:S(2)}, u32[]{:S(2)}) async-start(bf16[16,16,2048]{2,1,0:T(8,128)(2,1)} %broadcast_in_dim.56), calls=%async_computation | async-start | bytes 2097152 | tf_op jit(solution)/shard_map/all_to_all | solution.py:52
  21.2 0.7 convert_element_type.48
  21.8 0.1 compare_select_fusion
  21.9 0.7 fusion.43
  22.6 0.0 copy-start.6
  22.7 7.1 %attended.1 = bf16[8,16,256]{2,1,0:T(8,128)(2,1)} custom-call(s32[8]{0:T(128)} %lengths_ref.1, bf16[8,16,64]{2,1,0:T(8,128)(2,1)} %nope_ref.1, bf16[8,16,32]{2,1,0:T(8,128)(2,1)} %rope_ref.1, bf16[8,256]{1,0:T(8,128)(2,1)} %latent_ref.1, bf16[8,32]{1,0:T(8,128)(2,1)} %key_ref.1, f32[8,32]{1,0:T(8,128)} %get-tuple-element.22.cosine_ref, ...), custom_call_target="tpu_custom_call" | custom-call | flops 268435456 | bytes 4718592 | tf_op jit(solution)/shard_map/attended/pallas_call | solution.py:169
  29.8 0.0 copy-done.3
  29.8 1.3 fusion.2
  31.0 7.6 %all_gather.12 = bf16[16,2048]{1,0:T(8,128)(2,1)S(1)} all-gather(bf16[8,2048]{1,0:T(8,128)(2,1)S(1)} %fusion.2), channel_id=1, replica_groups=mesh['grp'=2,'ep_0'=8,'ep_1'=8,'tp'=2] {'tp'}, dimensions={0}, use_global_device_ids=true | all-gather | bytes 98304 | tf_op jit(solution)/shard_map/all_gather | solution.py:353
  38.6 0.0 collective-permute-start.2
  38.6 0.1 collective-permute-start.1
  38.8 2.5 %collective-permute-start = (bf16[16,2048]{1,0:T(8,128)(2,1)S(1)}, bf16[16,2048]{1,0:T(8,128)(2,1)S(1)}, u32[]{:S(2)}, u32[]{:S(2)}) collective-permute-start(bf16[16,2048]{1,0:T(8,128)(2,1)S(1)} %all_gather.12), channel_id=1, source_target_pairs={{0,2},{1,3},{2,0},{3,1},{4,6},{5,7},{6,4},{7,5},{8,10},{9,11},{10,... | collective-permute-start | bytes 196616 | tf_op jit(solution)/shard_map/ppermute | solution.py:48
  41.3 0.7 pad_add_fusion.place_ref
  42.0 7.9 %collective-permute-done.2 = bf16[16,2048]{1,0:T(8,128)(2,1)S(1)} collective-permute-done((bf16[16,2048]{1,0:T(8,128)(2,1)S(1)}, bf16[16,2048]{1,0:T(8,128)(2,1)S(1)}, u32[]{:S(2)}, u32[]{:S(2)}) %collective-permute-start.2) | collective-permute-done | bytes 65568 | tf_op jit(solution)/shard_map/ppermute | solution.py:48
  49.8 3.0 %collective-permute-done.1 = bf16[16,2048]{1,0:T(8,128)(2,1)S(1)} collective-permute-done((bf16[16,2048]{1,0:T(8,128)(2,1)S(1)}, bf16[16,2048]{1,0:T(8,128)(2,1)S(1)}, u32[]{:S(2)}, u32[]{:S(2)}) %collective-permute-start.1) | collective-permute-done | bytes 65568 | tf_op jit(solution)/shard_map/ppermute | solution.py:48
  52.8 0.0 collective-permute-done
  52.8 0.0 all-to-all-done
  52.8 1.7 %convolution_convert_fusion.2 = bf16[64,256]{1,0:T(8,128)(2,1)S(1)} fusion(bf16[256,2048]{1,0:T(8,128)(2,1)} %bitcast.9, bf16[16,2048]{1,0:T(8,128)(2,1)S(1)} %collective-permute-done.2, bf16[16,2048]{1,0:T(8,128)(2,1)S(1)} %collective-permute-done.1, bf16[16,2048]{1,0:T(8,128)(2,1)S(1)} %collective-permute-done, bf16[16,2048]{1,0:T(8,128)(2,1)S(1)} %all_gather.12), kind=kOutput, calls=%fused_computation.5 | convolution fusion | flops 68173824 | bytes 1343488 | tf_op jit(solution)/shard_map/dot_general | solution.py:357
  54.5 0.1 collective-permute-start.5
  54.6 0.1 collective-permute-start.4
  54.8 2.5 %collective-permute-start.3 = (bf16[16,256]{1,0:T(8,128)(2,1)S(1)}, bf16[16,256]{1,0:T(8,128)(2,1)S(1)}, u32[]{:S(2)}, u32[]{:S(2)}) collective-permute-start(bf16[16,256]{1,0:T(8,128)(2,1)S(1)} %get-tuple-element.18), channel_id=1, source_target_pairs={{0,2},{1,3},{2,0},{3,1},{4,6},{5,7},{6,4},{7,5},{8,10},{9,11},{10,... | collective-permute-start | bytes 24584 | tf_op jit(solution)/shard_map/ppermute | solution.py:48
  57.2 0.0 copy-done.6
  57.2 4.7 %all_gather.15.hidden_ref = bf16[16,2048]{1,0:T(8,128)(2,1)} all-gather(bf16[8,2048]{1,0:T(8,128)(2,1)S(1)} %copy-done.6), channel_id=1, replica_groups=mesh['grp'=2,'ep_0'=8,'ep_1'=8,'tp'=2] {'tp'}, dimensions={0}, use_global_device_ids=true | all-gather | bytes 98304 | tf_op jit(solution)/shard_map/all_gather | solution.py:341
  62.0 0.0 copy-done.8
  62.0 0.6 broadcast_in_dim.57.gain_mix_ref
  62.6 0.0 copy-done.9
  62.6 0.6 broadcast_in_dim.58.gain_in_ref
  63.2 0.0 copy-done.5
  63.2 0.7 copy.33.routes_ref
  63.9 0.0 collective-permute-done.5
  63.9 0.0 collective-permute-done.4
  63.9 0.0 collective-permute-done.3
  63.9 2.0 %all-gather = bf16[8,16,256]{2,1,0:T(8,128)(2,1)} all-gather(bf16[4,16,256]{2,1,0:T(8,128)(2,1)S(1)} %pad_maximum_fusion), channel_id=2, replica_groups=mesh['grp'=2,'ep_0'=8,'ep_1'=8,'tp'=2] {'tp'}, dimensions={0}, use_global_device_ids=true | all-gather | bytes 98304 | tf_op jit(solution)/shard_map/all_gather | solution.py:364
  65.9 2.4 %spread.1 = (bf16[128,2048]{1,0:T(8,128)(2,1)}, bf16[16,2048]{1,0:T(8,128)(2,1)}, bf16[8,2048]{1,0:T(8,128)(2,1)}, bf16[16,128]{1,0:T(8,128)(2,1)}) custom-call(s32[3]{0:T(128)} %pad_add_fusion.place_ref, bf16[2,4,16,256]{3,2,1,0:T(8,128)(2,1)} %bitcast.40, bf16[16,2048]{1,0:T(8,128)(2,1)} %all_gather.15.hidden_ref, ...), custom_call_target="tpu_custom_call" | custom-call | tf_op jit(solution)/shard_map/spread/pallas_call | solution.py:298
  68.4 1.4 %reshape.85 = bf16[64,2,2048]{2,1,0:T(2,128)(2,1)S(1)} reshape(bf16[128,2048]{1,0:T(8,128)(2,1)} %get-tuple-element.12) | data formatting | bytes 1048576 | tf_op jit(solution)/shard_map/reshape | solution.py:376
  69.8 27.2 %all_to_all.15 = bf16[64,2,2048]{2,1,0:T(2,128)(2,1)S(1)} all-to-all(bf16[64,2,2048]{2,1,0:T(2,128)(2,1)S(1)} %reshape.85), channel_id=1, replica_groups=mesh['grp'=2,'ep_0'=8,'ep_1'=8,'tp'=2] {'ep_0','ep_1'}, dimensions={0} | all-to-all | bytes 1048576 | tf_op jit(solution)/shard_map/all_to_all | solution.py:375
  97.0 0.2 reshape.86
  97.2 1.5 %fusion.10 = f32[128,256]{1,0:T(8,128)S(1)} fusion(bf16[128,2048]{1,0:T(8,128)(2,1)S(1)} %reshape.86, bf16[1,2048,256]{2,1,0:T(8,128)(2,1)} %param.37), kind=kOutput, calls=%fused_computation.16 | convolution fusion | flops 134217728 | bytes 1703936 | tf_op jit(solution)/shard_map/dot_general | solution.py:69
  98.7 0.0 copy-done
  98.7 0.0 copy-done.1
  98.7 0.8 convolution_convert_fusion
  99.5 0.0 copy-start.2
  99.5 0.0 copy-start.7
  99.5 1.1 reshape.87
  100.7 8.2 %all-to-all-start.2 = ((bf16[64,2,2048]{2,1,0:T(2,128)(2,1)}), bf16[64,2,2048]{2,1,0:T(2,128)(2,1)S(1)}, u32[]{:S(2)}, u32[]{:S(2)}) async-start(bf16[64,2,2048]{2,1,0:T(2,128)(2,1)} %reshape.87), calls=%async_computation.2 | async-start | bytes 1048576 | tf_op jit(solution)/shard_map/all_to_all | solution.py:396
  108.9 0.0 copy-done.10
  108.9 0.0 copy-done.4
  108.9 1.2 fusion.5
  110.2 0.2 select_reduce_fusion
  110.4 0.1 select_reduce_fusion.2
  110.5 0.0 copy-done.11
  110.5 13.4 %all-to-all-done.2 = bf16[64,2,2048]{2,1,0:T(2,128)(2,1)S(1)} async-done(((bf16[64,2,2048]{2,1,0:T(2,128)(2,1)}), bf16[64,2,2048]{2,1,0:T(2,128)(2,1)S(1)}, u32[]{:S(2)}, u32[]{:S(2)}) %all-to-all-start.2) | async-done | bytes 524320 | tf_op jit(solution)/shard_map/all_to_all | solution.py:396
  123.9 0.2 reshape.88
  124.1 0.2 fusion.33
  124.3 4.3 %collective-permute-start.6 = (f32[8,2048]{1,0:T(8,128)S(1)}, f32[8,2048]{1,0:T(8,128)S(1)}, u32[]{:S(2)}, u32[]{:S(2)}) collective-permute-start(f32[8,2048]{1,0:T(8,128)S(1)} %constant_dynamic-slice_fusion), channel_id=1, source_target_pairs={{0,1},{1,0},{2,3},{3,2},{4,5},{5,4},{6,7},{7,6},{8,9},{9,8},{10,11... | collective-permute-start | bytes 196616 | tf_op jit(solution)/shard_map/ppermute | solution.py:61
  128.7 1.5 %fusion.29 = f32[8,256]{1,0:T(8,128)S(1)} fusion(bf16[2048,256]{1,0:T(8,128)(2,1)} %param.40, bf16[16,2048]{1,0:T(8,128)(2,1)S(1)} %copy-done.4, s32[]{:T(128)S(6)} %select_n.49), kind=kOutput, calls=%fused_computation.43 | convolution fusion | flops 8388608 | bytes 1089540 | tf_op jit(solution)/shard_map/dot_general | solution.py:69
  130.2 0.0 collective-permute-done.6
  130.2 0.0 copy-done.2
  130.2 2.1 %multiply_reduce_fusion = (f32[8]{0:T(128)S(1)}, f32[8,2048]{1,0:T(8,128)S(1)}) fusion(bf16[256,2048]{1,0:T(8,128)(2,1)S(1)} %copy-done.2, bf16[2048,256]{1,0:T(8,128)(2,1)} %param.41, bf16[16,2048]{1,0:T(8,128)(2,1)S(1)} %copy-done.4, s32[]{:T(128)S(6)} %select_n.49, f32[8,256]{1,0:T(8,128)S(1)} %fusion.29, f32[8,2048]{1,0:T(8,128)S(1)} %collective-permute-done.6, ...), kind=kOutput, calls=%fused_computation.34 | convolution fusion | flops 16887800 | bytes 2335776 | tf_op jit(solution)/shard_map/dot_general | solution.py:72
  132.2 0.0 copy-done.7
  132.3 0.7 add_convert_fusion
  (17 shorter events, 0.1 us)
Async XLA Ops:
  0.0 98.7 %copy-start = (bf16[1,256,2048]{2,1,0:T(8,128)(2,1)S(1)}, bf16[1,256,2048]{2,1,0:T(8,128)(2,1)}, u32[]{:S(2)}) copy-start(bf16[1,256,2048]{2,1,0:T(8,128)(2,1)} %param.39) | copy-start | bytes 3145732
  0.0 29.8 %copy-start.3 = (bf16[256,16,128]{2,1,0:T(8,128)(2,1)S(1)}, bf16[256,16,128]{2,1,0:T(8,128)(2,1)}, u32[]{:S(2)}) copy-start(bf16[256,16,128]{2,1,0:T(8,128)(2,1)} %param.31) | copy-start | bytes 3145732
  2.1 50.7 %all-to-all-start = ((bf16[16,16,2048]{2,1,0:T(8,128)(2,1)}), bf16[16,16,2048]{2,1,0:T(8,128)(2,1)}, u32[]{:S(2)}, u32[]{:S(2)}) async-start(bf16[16,16,2048]{2,1,0:T(8,128)(2,1)} %broadcast_in_dim.56), calls=%async_computation | async-start | bytes 2097152 | tf_op jit(solution)/shard_map/all_to_all | solution.py:52
  22.6 34.6 %copy-start.6 = (bf16[8,2048]{1,0:T(8,128)(2,1)S(1)}, bf16[8,2048]{1,0:T(8,128)(2,1)}, u32[]{:S(2)}) copy-start(bf16[8,2048]{1,0:T(8,128)(2,1)} %param.22) | copy-start | bytes 98308
  22.6 39.3 %copy-start.8 = (bf16[2048]{0:T(1024)(128)(2,1)S(1)}, bf16[2048]{0:T(1024)(128)(2,1)}, u32[]{:S(2)}) copy-start(bf16[2048]{0:T(1024)(128)(2,1)} %param.33) | copy-start | bytes 12292
  22.6 39.9 %copy-start.9 = (bf16[2048]{0:T(1024)(128)(2,1)S(1)}, bf16[2048]{0:T(1024)(128)(2,1)}, u32[]{:S(2)}) copy-start(bf16[2048]{0:T(1024)(128)(2,1)} %param.34) | copy-start | bytes 12292
  22.6 40.5 %copy-start.5 = (s32[16,6]{0,1:T(8,128)S(1)}, s32[16,6]{0,1:T(8,128)}, u32[]{:S(2)}) copy-start(s32[16,6]{0,1:T(8,128)} %param.36) | copy-start | bytes 1156
  29.8 69.0 %copy-start.1 = (bf16[1,2048,256]{2,1,0:T(8,128)(2,1)S(1)}, bf16[1,2048,256]{2,1,0:T(8,128)(2,1)}, u32[]{:S(2)}) copy-start(bf16[1,2048,256]{2,1,0:T(8,128)(2,1)} %param.38) | copy-start | bytes 3145732
  38.6 11.2 %collective-permute-start.2 = (bf16[16,2048]{1,0:T(8,128)(2,1)S(1)}, bf16[16,2048]{1,0:T(8,128)(2,1)S(1)}, u32[]{:S(2)}, u32[]{:S(2)}) collective-permute-start(bf16[16,2048]{1,0:T(8,128)(2,1)S(1)} %all_gather.12), channel_id=1, source_target_pairs={{0,18},{1,19},{2,16},{3,17},{4,22},{5,23},{6,20},{7,21},{8,26},{9,... | collective-permute-start | bytes 196616 | tf_op jit(solution)/shard_map/ppermute | solution.py:48
  38.6 14.1 %collective-permute-start.1 = (bf16[16,2048]{1,0:T(8,128)(2,1)S(1)}, bf16[16,2048]{1,0:T(8,128)(2,1)S(1)}, u32[]{:S(2)}, u32[]{:S(2)}) collective-permute-start(bf16[16,2048]{1,0:T(8,128)(2,1)S(1)} %all_gather.12), channel_id=1, source_target_pairs={{0,16},{1,17},{2,18},{3,19},{4,20},{5,21},{6,22},{7,23},{8,24},{9,... | collective-permute-start | bytes 196616 | tf_op jit(solution)/shard_map/ppermute | solution.py:48
  38.8 14.0 %collective-permute-start = (bf16[16,2048]{1,0:T(8,128)(2,1)S(1)}, bf16[16,2048]{1,0:T(8,128)(2,1)S(1)}, u32[]{:S(2)}, u32[]{:S(2)}) collective-permute-start(bf16[16,2048]{1,0:T(8,128)(2,1)S(1)} %all_gather.12), channel_id=1, source_target_pairs={{0,2},{1,3},{2,0},{3,1},{4,6},{5,7},{6,4},{7,5},{8,10},{9,11},{10,... | collective-permute-start | bytes 196616 | tf_op jit(solution)/shard_map/ppermute | solution.py:48
  54.5 9.4 %collective-permute-start.5 = (bf16[16,256]{1,0:T(8,128)(2,1)S(1)}, bf16[16,256]{1,0:T(8,128)(2,1)S(1)}, u32[]{:S(2)}, u32[]{:S(2)}) collective-permute-start(bf16[16,256]{1,0:T(8,128)(2,1)S(1)} %get-tuple-element.16), channel_id=1, source_target_pairs={{0,18},{1,19},{2,16},{3,17},{4,22},{5,23},{6,20},{7,21},{8,26},{9,... | collective-permute-start | bytes 24584 | tf_op jit(solution)/shard_map/ppermute | solution.py:48
  54.6 9.3 %collective-permute-start.4 = (bf16[16,256]{1,0:T(8,128)(2,1)S(1)}, bf16[16,256]{1,0:T(8,128)(2,1)S(1)}, u32[]{:S(2)}, u32[]{:S(2)}) collective-permute-start(bf16[16,256]{1,0:T(8,128)(2,1)S(1)} %get-tuple-element.17), channel_id=1, source_target_pairs={{0,16},{1,17},{2,18},{3,19},{4,20},{5,21},{6,22},{7,23},{8,24},{9,... | collective-permute-start | bytes 24584 | tf_op jit(solution)/shard_map/ppermute | solution.py:48
  54.8 9.1 %collective-permute-start.3 = (bf16[16,256]{1,0:T(8,128)(2,1)S(1)}, bf16[16,256]{1,0:T(8,128)(2,1)S(1)}, u32[]{:S(2)}, u32[]{:S(2)}) collective-permute-start(bf16[16,256]{1,0:T(8,128)(2,1)S(1)} %get-tuple-element.18), channel_id=1, source_target_pairs={{0,2},{1,3},{2,0},{3,1},{4,6},{5,7},{6,4},{7,5},{8,10},{9,11},{10,... | collective-permute-start | bytes 24584 | tf_op jit(solution)/shard_map/ppermute | solution.py:48
  96.9 11.9 %copy-start.10 = (bf16[2048]{0:T(1024)(128)(2,1)S(1)}, bf16[2048]{0:T(1024)(128)(2,1)}, u32[]{:S(2)}) copy-start(bf16[2048]{0:T(1024)(128)(2,1)} %param.43) | copy-start | bytes 12292
  97.0 12.0 %copy-start.4 = (bf16[16,2048]{1,0:T(8,128)(2,1)S(1)}, bf16[16,2048]{1,0:T(8,128)(2,1)}, u32[]{:S(2)}) copy-start(bf16[16,2048]{1,0:T(8,128)(2,1)} %get-tuple-element.10) | copy-start | bytes 196612
  97.0 13.5 %copy-start.11 = (bf16[16,128]{1,0:T(8,128)(2,1)S(1)}, bf16[16,128]{1,0:T(8,128)(2,1)}, u32[]{:S(2)}) copy-start(bf16[16,128]{1,0:T(8,128)(2,1)} %get-tuple-element.11) | copy-start | bytes 12292
  99.5 30.7 %copy-start.2 = (bf16[256,2048]{1,0:T(8,128)(2,1)S(1)}, bf16[256,2048]{1,0:T(8,128)(2,1)}, u32[]{:S(2)}) copy-start(bf16[256,2048]{1,0:T(8,128)(2,1)} %param.42) | copy-start | bytes 3145732
  99.5 32.7 %copy-start.7 = (bf16[8,2048]{1,0:T(8,128)(2,1)S(1)}, bf16[8,2048]{1,0:T(8,128)(2,1)}, u32[]{:S(2)}) copy-start(bf16[8,2048]{1,0:T(8,128)(2,1)} %get-tuple-element.9) | copy-start | bytes 98308
  100.7 23.2 %all-to-all-start.2 = ((bf16[64,2,2048]{2,1,0:T(2,128)(2,1)}), bf16[64,2,2048]{2,1,0:T(2,128)(2,1)S(1)}, u32[]{:S(2)}, u32[]{:S(2)}) async-start(bf16[64,2,2048]{2,1,0:T(2,128)(2,1)} %reshape.87), calls=%async_computation.2 | async-start | bytes 1048576 | tf_op jit(solution)/shard_map/all_to_all | solution.py:396
  124.3 5.8 %collective-permute-start.6 = (f32[8,2048]{1,0:T(8,128)S(1)}, f32[8,2048]{1,0:T(8,128)S(1)}, u32[]{:S(2)}, u32[]{:S(2)}) collective-permute-start(f32[8,2048]{1,0:T(8,128)S(1)} %constant_dynamic-slice_fusion), channel_id=1, source_target_pairs={{0,1},{1,0},{2,3},{3,2},{4,5},{5,4},{6,7},{7,6},{8,9},{9,8},{10,11... | collective-permute-start | bytes 196616 | tf_op jit(solution)/shard_map/ppermute | solution.py:61
where the time goes:
time: 134 us; the launch traced here: 133 us
  blocking collectives  41.6 us (31%)
  starting transfers between devices  37 us (28%)
  waiting for transfers between devices  24.2 us (18%)
  matrix products  10.2 us (8%)
  Pallas kernels  9.54 us (7%)
  local copies, waits for them, and re-layouts  6.97 us (5%)
  other arithmetic  3.19 us (2%)
    all_to_all x1, blocking collectives, local(): lax.all_to_all(outgoing.reshape(ep_count, capacity, width), EP, split_axi...  27.2 us
    all_to_all x1, starting transfers between devices, exchanged(): lax.all_to_all(blocks, EP_TP, 0, 0, axis_index_groups=groups, tiled=True)  19.1 us
    all_to_all x1, waiting for transfers between devices, local(): lax.all_to_all(outputs.reshape(ep_count, capacity, width), EP, split_axis...  13.4 us
    ppermute x6, waiting for transfers between devices, from_partner(): return lax.ppermute(array, EP_TP, partners(flip // 2, flip % 2))  10.8 us
    all_to_all x1, starting transfers between devices, local(): lax.all_to_all(outputs.reshape(ep_count, capacity, width), EP, split_axis...  8.19 us
    all_gather x1, blocking collectives, local(): chip_heads = lax.all_gather(heads_out, 'tp', axis=0, tiled=True)  7.61 us
    pallas_call x1, Pallas kernels, attended(): pl.pallas_call(attention_kernel, grid_spec=pltpu.PrefetchScalarGridSpec(n...  7.1 us
    ppermute x6, starting transfers between devices, from_partner(): return lax.ppermute(array, EP_TP, partners(flip // 2, flip % 2))  5.4 us
  transfers between devices with their start and end apart: 9, of which 3 were waited for; matrix products, arithmetic and copies ran while one was open for 6% of the time, Pallas kernels for 5%

commit v1 on v0

--- a/solution.py
+++ b/solution.py
@@ -191,7 +191,7 @@
             ],
         ),
         out_shape=jax.ShapeDtypeStruct((seq_count, heads, latent), jnp.bfloat16),
-        compiler_params=pltpu.CompilerParams(dimension_semantics=("arbitrary",)),
+        compiler_params=pltpu.CompilerParams(dimension_semantics=("arbitrary",), vmem_limit_bytes=60 * 1024 * 1024),
         cost_estimate=pl.CostEstimate(
             flops=8 * seq_count * heads * context * latent,
             bytes_accessed=2 * seq_count * context * (latent + rope),
@@ -266,31 +266,30 @@
     )
     after_mix = (
         hidden_ref[...].astype(jnp.float32)
-        + gain_mix_ref[...].astype(jnp.float32) * normalize(mixed)
+        + gain_mix_ref[...].astype(jnp.float32)[None] * normalize(mixed)
     ).astype(jnp.bfloat16)
     after_wide = after_mix.astype(jnp.float32)
-    ffn_in = (normalize(after_wide) * gain_in_ref[...].astype(jnp.float32)).astype(jnp.bfloat16)
+    ffn_in = (normalize(after_wide) * gain_in_ref[...].astype(jnp.float32)[None]).astype(jnp.bfloat16)
     ffn_ref[...] = ffn_in
     half = rows // 2
     mix_ref[...] = jnp.where(core == 0, after_wide[:half], after_wide[half:]).astype(jnp.bfloat16)
-    slots = outgoing_ref.shape[0]
-    slot = lax.broadcasted_iota(jnp.int32, (rows, slots), 1)
+    slots = taken_ref.shape[0]
+    slot = lax.broadcasted_iota(jnp.int32, (slots, rows), 0)
     expert = slot // 2 * 2 + core
-    named = jnp.zeros((rows, slots), jnp.float32)
-    for n in range(routes_ref.shape[1]):
-        named = jnp.where(routes_ref[:, n : n + 1] == expert, 1.0, named)
+    named = jnp.zeros((slots, rows), jnp.float32)
+    for n in range(routes_ref.shape[0]):
+        named = jnp.where(routes_ref[n : n + 1, :] == expert, 1.0, named)
     earlier = jnp.where(
-        lax.broadcasted_iota(jnp.int32, (rows, rows), 1)
-        < lax.broadcasted_iota(jnp.int32, (rows, rows), 0),
+        lax.broadcasted_iota(jnp.int32, (rows, rows), 0)
+        < lax.broadcasted_iota(jnp.int32, (rows, rows), 1),
         1.0,
         0.0,
     ).astype(jnp.bfloat16)
-    before = jnp.dot(earlier, named.astype(jnp.bfloat16), preferred_element_type=jnp.float32)
+    before = jnp.dot(named.astype(jnp.bfloat16), earlier, preferred_element_type=jnp.float32)
     taken = jnp.where(before == (slot % 2).astype(jnp.float32), named, 0.0).astype(jnp.bfloat16)
     taken_ref[...] = taken
-    outgoing_ref[...] = lax.dot_general(
-        taken, ffn_in, (((0,), (0,)), ((), ())), preferred_element_type=jnp.float32
-    ).astype(jnp.bfloat16)
+    outgoing = jnp.dot(taken, ffn_in, preferred_element_type=jnp.float32).astype(jnp.bfloat16)
+    outgoing_ref[...] = outgoing.reshape(outgoing_ref.shape)
 
 
 def spread(place, pieces, chip_hidden, gain_mix, gain_in, routes, slots):
@@ -301,13 +300,34 @@
         + [pl.BlockSpec(memory_space=pltpu.VMEM)] * 5,
         out_specs=[pl.BlockSpec(memory_space=pltpu.VMEM)] * 4,
         out_shape=[
-            jax.ShapeDtypeStruct((slots, width), jnp.bfloat16),
+            jax.ShapeDtypeStruct((slots // 2, 2, width), jnp.bfloat16),
             jax.ShapeDtypeStruct((rows, width), jnp.bfloat16),
             jax.ShapeDtypeStruct((rows // 2, width), jnp.bfloat16),
-            jax.ShapeDtypeStruct((rows, slots), jnp.bfloat16),
+            jax.ShapeDtypeStruct((slots, rows), jnp.bfloat16),
         ],
+        compiler_params=pltpu.CompilerParams(vmem_limit_bytes=8 << 20),
         name="spread",
-    )(place, pieces, chip_hidden, gain_mix[None], gain_in[None], routes)
+    )(place, pieces, chip_hidden, gain_mix, gain_in, routes.T)
+
+
+def experts_kernel(rows_ref, gate_ref, up_ref, down_ref, out_ref):
+    rows = rows_ref[...]
+    gate_part = jnp.dot(rows, gate_ref[...], preferred_element_type=jnp.float32)
+    up_part = jnp.dot(rows, up_ref[...], preferred_element_type=jnp.float32)
+    inner = (gate_part / (1.0 + jnp.exp(-gate_part)) * up_part).astype(jnp.bfloat16)
+    out_ref[...] = jnp.dot(inner, down_ref[...], preferred_element_type=jnp.float32).astype(
+        out_ref.dtype
+    )
+
+
+def expert_rows(rows, gate_w, up_w, down_w):
+    return pl.pallas_call(
+        experts_kernel,
+        in_specs=[pl.BlockSpec(memory_space=pltpu.VMEM)] * 4,
+        out_specs=pl.BlockSpec(memory_space=pltpu.VMEM),
+        out_shape=jax.ShapeDtypeStruct((rows.shape[0], down_w.shape[1]), jnp.bfloat16),
+        compiler_params=pltpu.CompilerParams(vmem_limit_bytes=10 << 20),
+    )(rows, gate_w, up_w, down_w)
 
 
 def local(
@@ -373,7 +393,7 @@
         place.astype(jnp.int32), pieces, chip_hidden, gain_mix, gain_ffn_in, routes, slots
     )
     received = lax.all_to_all(
-        outgoing.reshape(ep_count, capacity, width), EP, split_axis=0, concat_axis=0, tiled=True
+        outgoing, EP, split_axis=0, concat_axis=0, tiled=True
     )
     affinity = jax.nn.sigmoid(jnp.dot(ffn_in, router, preferred_element_type=jnp.float32))
     choose = routes[..., None] == lax.iota(jnp.int32, experts_total)[None, None, :]
@@ -385,11 +405,11 @@
         ),
         axis=1,
     )
-    slot_weights = slot_weights * taken.astype(jnp.float32)
+    slot_weights = slot_weights * taken.T.astype(jnp.float32)
     weights_high = slot_weights.astype(jnp.bfloat16)
     weights_low = (slot_weights - weights_high.astype(jnp.float32)).astype(jnp.bfloat16)
     own_ffn = lax.dynamic_slice_in_dim(ffn_in, own_start, seq_count, 0)
-    shared = swiglu(own_ffn, shared_gate, shared_up, shared_down)
+    shared = expert_rows(own_ffn, shared_gate, shared_up, shared_down)
     outputs = swiglu(
         received.reshape(slots, width), expert_gate[0], expert_up[0], expert_down[0]
     )

time: 134 us -> 135 us (level)
  blocking collectives: 41.6 us -> 13.7 us
  waiting for transfers between devices: 24.2 us -> 41.6 us
  starting transfers between devices: 37 us -> 48.4 us
  local copies, waits for them, and re-layouts: 6.97 us -> 8.83 us
  matrix products: 10.2 us -> 8.73 us
    all_to_all x1 -> x0, blocking collectives: 27.2 us -> none  [local(): lax.all_to_all(outgoing.reshape(ep_count, capacity, width), EP, split_axi...]
    all_to_all x0 -> x1, waiting for transfers between devices: none -> 16.2 us  [local(): lax.all_to_all(outgoing, EP, split_axis=0, concat_axis=0, tiled=True)]
    all_to_all x0 -> x1, starting transfers between devices: none -> 11.3 us  [local(): lax.all_to_all(outgoing, EP, split_axis=0, concat_axis=0, tiled=True)]
    reshape x1, local copies, waits for them, and re-layouts: 0.2 us -> 2.04 us  [local(): returned = lax.all_to_all(outputs.reshape(ep_count, capacity, width), EP,...]
    dot_general x2 -> x1, matrix products: 3 us -> 1.54 us  [swiglu(): gate_part = jnp.dot(flat_rows, gate_w, preferred_element_type=jnp.float32)]
    ppermute x6, waiting for transfers between devices: 10.8 us -> 12.2 us  [from_partner(): return lax.ppermute(array, EP_TP, partners(flip // 2, flip % 2))]
    reshape x1 -> x0, local copies, waits for them, and re-layouts: 1.38 us -> none  [local(): outgoing.reshape(ep_count, capacity, width)]
    dot_general x2 -> x1, matrix products: 2.84 us -> 3.1 us  [swiglu(): jnp.dot(inner_rows, down_w, preferred_element_type=jnp.float32)]
  transfers between devices with their start and end apart: 9 -> 10, of which waited for: 3 -> 4; matrix products, arithmetic and copies ran while one was open for 6% -> 3% of each run, Pallas kernels for 5% -> 6%
where the time goes in v1:
time: 135 us; the launch traced here: 134 us
  starting transfers between devices  48.4 us (36%)
  waiting for transfers between devices  41.6 us (31%)
  blocking collectives  13.7 us (10%)
  Pallas kernels  9.78 us (7%)
  local copies, waits for them, and re-layouts  8.83 us (7%)
  matrix products  8.73 us (6%)
  other arithmetic  2.8 us (2%)
    all_to_all x1, starting transfers between devices, exchanged(): lax.all_to_all(blocks, EP_TP, 0, 0, axis_index_groups=groups, tiled=True)  19.1 us
    all_to_all x1, waiting for transfers between devices, local(): lax.all_to_all(outgoing, EP, split_axis=0, concat_axis=0, tiled=True)  16.2 us
    all_to_all x1, waiting for transfers between devices, local(): lax.all_to_all(outputs.reshape(ep_count, capacity, width), EP, split_axis...  13.1 us
    ppermute x6, waiting for transfers between devices, from_partner(): return lax.ppermute(array, EP_TP, partners(flip // 2, flip % 2))  12.2 us
    all_to_all x1, starting transfers between devices, local(): lax.all_to_all(outgoing, EP, split_axis=0, concat_axis=0, tiled=True)  11.3 us
    all_to_all x1, starting transfers between devices, local(): lax.all_to_all(outputs.reshape(ep_count, capacity, width), EP, split_axis...  8.23 us
    pallas_call x1, Pallas kernels, attended(): pl.pallas_call(attention_kernel, grid_spec=pltpu.PrefetchScalarGridSpec(n...  7.1 us
    all_gather x1, blocking collectives, local(): chip_heads = lax.all_gather(heads_out, 'tp', axis=0, tiled=True)  6.98 us
  transfers between devices with their start and end apart: 10, of which 4 were waited for; matrix products, arithmetic and copies ran while one was open for 3% of the time, Pallas kernels for 6%

profile of v1, /device:TPU:513, one launch (start us, length us, event | category | flops | bytes accessed | tf_op | source)
XLA Modules:
  0.0 134.1 jit_solution(11379137857221441734)
XLA Ops:
  0.0 0.0 copy-start
  0.0 2.1 %broadcast_in_dim.34 = bf16[16,16,2048]{2,1,0:T(8,128)(2,1)} broadcast(bf16[16,2048]{1,0:T(8,128)(2,1)} %bitcast.49), dimensions={1,2} | broadcast | bytes 1114112 | tf_op jit(solution)/shard_map/broadcast_in_dim | solution.py:57
  2.1 19.1 %all-to-all-start = ((bf16[16,16,2048]{2,1,0:T(8,128)(2,1)}), bf16[16,16,2048]{2,1,0:T(8,128)(2,1)S(1)}, u32[]{:S(2)}, u32[]{:S(2)}) async-start(bf16[16,16,2048]{2,1,0:T(8,128)(2,1)} %broadcast_in_dim.34), calls=%async_computation | async-start | bytes 2097152 | tf_op jit(solution)/shard_map/all_to_all | solution.py:52
  21.2 0.7 convert_element_type.45
  21.8 0.1 compare_select_fusion
  21.9 0.7 fusion.30
  22.6 0.0 copy-start.10
  22.7 7.1 %attended.1 = bf16[8,16,256]{2,1,0:T(8,128)(2,1)} custom-call(s32[8]{0:T(128)} %lengths_ref.1, bf16[8,16,64]{2,1,0:T(8,128)(2,1)} %nope_ref.1, bf16[8,16,32]{2,1,0:T(8,128)(2,1)} %rope_ref.1, bf16[8,256]{1,0:T(8,128)(2,1)} %latent_ref.1, bf16[8,32]{1,0:T(8,128)(2,1)} %key_ref.1, f32[8,32]{1,0:T(8,128)} %get-tuple-element.20.cosine_ref, ...), custom_call_target="tpu_custom_call" | custom-call | flops 268435456 | bytes 4718592 | tf_op jit(solution)/shard_map/attended/pallas_call | solution.py:169
  29.8 0.0 copy-done.8
  29.8 1.2 fusion.1
  30.9 7.0 %all_gather.12 = bf16[16,2048]{1,0:T(8,128)(2,1)S(1)} all-gather(bf16[8,2048]{1,0:T(8,128)(2,1)S(1)} %fusion.1), channel_id=1, replica_groups=mesh['grp'=2,'ep_0'=8,'ep_1'=8,'tp'=2] {'tp'}, dimensions={0}, use_global_device_ids=true | all-gather | bytes 98304 | tf_op jit(solution)/shard_map/all_gather | solution.py:373
  37.9 0.0 collective-permute-start.2
  37.9 0.1 collective-permute-start.1
  38.1 2.5 %collective-permute-start = (bf16[16,2048]{1,0:T(8,128)(2,1)S(1)}, bf16[16,2048]{1,0:T(8,128)(2,1)S(1)}, u32[]{:S(2)}, u32[]{:S(2)}) collective-permute-start(bf16[16,2048]{1,0:T(8,128)(2,1)S(1)} %all_gather.12), channel_id=1, source_target_pairs={{0,2},{1,3},{2,0},{3,1},{4,6},{5,7},{6,4},{7,5},{8,10},{9,11},{10,... | collective-permute-start | bytes 196616 | tf_op jit(solution)/shard_map/ppermute | solution.py:48
  40.6 0.1 pad_add_fusion.place_ref
  40.6 9.0 %collective-permute-done.2 = bf16[16,2048]{1,0:T(8,128)(2,1)S(1)} collective-permute-done((bf16[16,2048]{1,0:T(8,128)(2,1)S(1)}, bf16[16,2048]{1,0:T(8,128)(2,1)S(1)}, u32[]{:S(2)}, u32[]{:S(2)}) %collective-permute-start.2) | collective-permute-done | bytes 65568 | tf_op jit(solution)/shard_map/ppermute | solution.py:48
  49.6 3.2 %collective-permute-done.1 = bf16[16,2048]{1,0:T(8,128)(2,1)S(1)} collective-permute-done((bf16[16,2048]{1,0:T(8,128)(2,1)S(1)}, bf16[16,2048]{1,0:T(8,128)(2,1)S(1)}, u32[]{:S(2)}, u32[]{:S(2)}) %collective-permute-start.1) | collective-permute-done | bytes 65568 | tf_op jit(solution)/shard_map/ppermute | solution.py:48
  52.9 0.0 collective-permute-done
  52.9 0.0 all-to-all-done
  52.9 0.4 convolution_convert_fusion.1
  53.3 0.1 collective-permute-start.5
  53.5 0.1 collective-permute-start.4
  53.6 2.5 %collective-permute-start.3 = (bf16[16,256]{1,0:T(8,128)(2,1)S(1)}, bf16[16,256]{1,0:T(8,128)(2,1)S(1)}, u32[]{:S(2)}, u32[]{:S(2)}) collective-permute-start(bf16[16,256]{1,0:T(8,128)(2,1)S(1)} %get-tuple-element.18), channel_id=1, source_target_pairs={{0,2},{1,3},{2,0},{3,1},{4,6},{5,7},{6,4},{7,5},{8,10},{9,11},{10,... | collective-permute-start | bytes 24584 | tf_op jit(solution)/shard_map/ppermute | solution.py:48
  56.1 0.0 copy-done.9
  56.1 4.4 %all_gather.15.hidden_ref = bf16[16,2048]{1,0:T(8,128)(2,1)S(1)} all-gather(bf16[8,2048]{1,0:T(8,128)(2,1)S(1)} %copy-done.9), channel_id=1, replica_groups=mesh['grp'=2,'ep_0'=8,'ep_1'=8,'tp'=2] {'tp'}, dimensions={0}, use_global_device_ids=true | all-gather | bytes 98304 | tf_op jit(solution)/shard_map/all_gather | solution.py:361
  60.5 0.0 collective-permute-done.5
  60.5 0.0 collective-permute-done.4
  60.5 0.0 collective-permute-done.3
  60.5 2.3 %all-gather = bf16[8,16,256]{2,1,0:T(8,128)(2,1)S(1)} all-gather(bf16[4,16,256]{2,1,0:T(8,128)(2,1)S(1)} %pad_maximum_fusion), channel_id=2, replica_groups=mesh['grp'=2,'ep_0'=8,'ep_1'=8,'tp'=2] {'tp'}, dimensions={0}, use_global_device_ids=true | all-gather | bytes 98304 | tf_op jit(solution)/shard_map/all_gather | solution.py:384
  62.8 0.0 copy-done.4
  62.8 0.0 copy-done.5
  62.8 0.0 copy-done.6
  62.8 2.1 %spread.1 = (bf16[64,2,2048]{2,1,0:T(2,128)(2,1)}, bf16[16,2048]{1,0:T(8,128)(2,1)S(1)}, bf16[8,2048]{1,0:T(8,128)(2,1)S(1)}, bf16[128,16]{1,0:T(8,128)(2,1)S(1)}) custom-call(s32[3]{0:T(128)S(1)} %pad_add_fusion.place_ref, bf16[2,4,16,256]{3,2,1,0:T(8,128)(2,1)S(1)} %bitcast.44, bf16[16,2048]{1,0:T(8,128)(2,1)S(1)} %all_gather.15.hidden_ref, ...), custom_call_target="tpu_custom_call" | custom-call | tf_op jit(solution)/shard_map/spread/pallas_call | solution.py:297
  64.9 11.3 %all-to-all-start.1 = ((bf16[64,2,2048]{2,1,0:T(2,128)(2,1)}), bf16[64,2,2048]{2,1,0:T(2,128)(2,1)S(1)}, u32[]{:S(2)}, u32[]{:S(2)}) async-start(bf16[64,2,2048]{2,1,0:T(2,128)(2,1)} %get-tuple-element.12), calls=%async_computation.1 | async-start | bytes 1048576 | tf_op jit(solution)/shard_map/all_to_all | solution.py:395
  76.3 0.0 copy-done.10
  76.3 16.2 %all-to-all-done.1 = bf16[64,2,2048]{2,1,0:T(2,128)(2,1)S(1)} async-done(((bf16[64,2,2048]{2,1,0:T(2,128)(2,1)}), bf16[64,2,2048]{2,1,0:T(2,128)(2,1)S(1)}, u32[]{:S(2)}, u32[]{:S(2)}) %all-to-all-start.1) | async-done | bytes 524320 | tf_op jit(solution)/shard_map/all_to_all | solution.py:395
  92.5 0.2 reshape.82
  92.7 0.0 copy-start.7
  92.7 0.8 copy-done.7
  93.5 1.5 %fusion.8 = f32[128,256]{1,0:T(8,128)S(1)} fusion(bf16[128,2048]{1,0:T(8,128)(2,1)S(1)} %reshape.82, bf16[1,2048,256]{2,1,0:T(8,128)(2,1)} %param.37), kind=kOutput, calls=%fused_computation.12 | convolution fusion | flops 134217728 | bytes 1703936 | tf_op jit(solution)/shard_map/dot_general | solution.py:69
  95.0 0.0 copy-done
  95.0 0.0 copy-start.1
  95.0 0.0 copy-start.2
  95.0 3.1 %convolution_convert_fusion = bf16[128,2048]{1,0:T(8,128)(2,1)} fusion(bf16[128,2048]{1,0:T(8,128)(2,1)} %copy-done.7, bf16[1,256,2048]{2,1,0:T(8,128)(2,1)S(1)} %copy-done, bf16[1,2048,256]{2,1,0:T(8,128)(2,1)} %param.38, f32[128,256]{1,0:T(8,128)S(1)} %fusion.8), kind=kOutput, calls=%fused_computation | convolution fusion | flops 268894208 | bytes 3276800 | tf_op jit(solution)/shard_map/dot_general | solution.py:72
  98.1 2.2 %reshape.83 = bf16[64,2,2048]{2,1,0:T(2,128)(2,1)} reshape(bf16[128,2048]{1,0:T(8,128)(2,1)} %convolution_convert_fusion) | data formatting | bytes 1048576 | tf_op jit(solution)/shard_map/reshape | solution.py:417
  100.3 8.2 %all-to-all-start.2 = ((bf16[64,2,2048]{2,1,0:T(2,128)(2,1)}), bf16[64,2,2048]{2,1,0:T(2,128)(2,1)}, u32[]{:S(2)}, u32[]{:S(2)}) async-start(bf16[64,2,2048]{2,1,0:T(2,128)(2,1)} %reshape.83), calls=%async_computation.2 | async-start | bytes 1048576 | tf_op jit(solution)/shard_map/all_to_all | solution.py:416
  108.6 1.2 fusion.4
  109.8 0.2 select_reduce_fusion
  110.0 0.1 select_reduce_fusion.2
  110.1 0.1 copy.38
  110.3 0.1 copy.39
  110.4 0.1 copy.40
  110.4 13.1 %all-to-all-done.2 = bf16[64,2,2048]{2,1,0:T(2,128)(2,1)} async-done(((bf16[64,2,2048]{2,1,0:T(2,128)(2,1)}), bf16[64,2,2048]{2,1,0:T(2,128)(2,1)}, u32[]{:S(2)}, u32[]{:S(2)}) %all-to-all-start.2) | async-done | bytes 524320 | tf_op jit(solution)/shard_map/all_to_all | solution.py:416
  123.6 2.0 %reshape.84 = bf16[128,2048]{1,0:T(8,128)(2,1)} reshape(bf16[64,2,2048]{2,1,0:T(2,128)(2,1)} %all-to-all-done.2) | data formatting | bytes 1048576 | tf_op jit(solution)/shard_map/reshape | solution.py:418
  125.6 1.2 fusion.26
  126.9 4.4 %collective-permute-start.6 = (f32[8,2048]{1,0:T(8,128)S(1)}, f32[8,2048]{1,0:T(8,128)S(1)}, u32[]{:S(2)}, u32[]{:S(2)}) collective-permute-start(f32[8,2048]{1,0:T(8,128)S(1)} %constant_dynamic-slice_fusion.1), channel_id=1, source_target_pairs={{0,1},{1,0},{2,3},{3,2},{4,5},{5,4},{6,7},{7,6},{8,9},{9,8},{10,11... | collective-permute-start | bytes 196616 | tf_op jit(solution)/shard_map/ppermute | solution.py:61
  131.4 0.0 copy-done.1
  131.4 0.0 copy-done.2
  131.4 0.0 copy-start.3
  131.4 1.2 copy-done.3
  132.6 0.6 shard_map.208
  133.2 0.0 collective-permute-done.6
  133.2 0.1 multiply_reduce_fusion
  133.4 0.7 add_convert_fusion
  (17 shorter events, 0.1 us)
Async XLA Ops:
  0.0 95.0 %copy-start = (bf16[1,256,2048]{2,1,0:T(8,128)(2,1)S(1)}, bf16[1,256,2048]{2,1,0:T(8,128)(2,1)}, u32[]{:S(2)}) copy-start(bf16[1,256,2048]{2,1,0:T(8,128)(2,1)} %param.39) | copy-start | bytes 3145732
  0.0 29.8 %copy-start.8 = (bf16[256,16,128]{2,1,0:T(8,128)(2,1)S(1)}, bf16[256,16,128]{2,1,0:T(8,128)(2,1)}, u32[]{:S(2)}) copy-start(bf16[256,16,128]{2,1,0:T(8,128)(2,1)} %param.31) | copy-start | bytes 3145732
  2.1 50.8 %all-to-all-start = ((bf16[16,16,2048]{2,1,0:T(8,128)(2,1)}), bf16[16,16,2048]{2,1,0:T(8,128)(2,1)S(1)}, u32[]{:S(2)}, u32[]{:S(2)}) async-start(bf16[16,16,2048]{2,1,0:T(8,128)(2,1)} %broadcast_in_dim.34), calls=%async_computation | async-start | bytes 2097152 | tf_op jit(solution)/shard_map/all_to_all | solution.py:52
  22.6 33.5 %copy-start.9 = (bf16[8,2048]{1,0:T(8,128)(2,1)S(1)}, bf16[8,2048]{1,0:T(8,128)(2,1)}, u32[]{:S(2)}) copy-start(bf16[8,2048]{1,0:T(8,128)(2,1)} %param.22) | copy-start | bytes 98308
  22.6 40.2 %copy-start.4 = (s32[16,6]{0,1:T(8,128)S(1)}, s32[16,6]{0,1:T(8,128)}, u32[]{:S(2)}) copy-start(s32[16,6]{0,1:T(8,128)} %param.36) | copy-start | bytes 1156
  22.6 40.2 %copy-start.5 = (bf16[2048]{0:T(1024)(128)(2,1)S(1)}, bf16[2048]{0:T(1024)(128)(2,1)}, u32[]{:S(2)}) copy-start(bf16[2048]{0:T(1024)(128)(2,1)} %gain_mix_ref.1) | copy-start | bytes 12292
  22.6 40.2 %copy-start.6 = (bf16[2048]{0:T(1024)(128)(2,1)S(1)}, bf16[2048]{0:T(1024)(128)(2,1)}, u32[]{:S(2)}) copy-start(bf16[2048]{0:T(1024)(128)(2,1)} %gain_in_ref.1) | copy-start | bytes 12292
  22.6 53.6 %copy-start.10 = (bf16[2048]{0:T(1024)(128)(2,1)S(1)}, bf16[2048]{0:T(1024)(128)(2,1)}, u32[]{:S(2)}) copy-start(bf16[2048]{0:T(1024)(128)(2,1)} %param.43) | copy-start | bytes 12292
  37.9 11.7 %collective-permute-start.2 = (bf16[16,2048]{1,0:T(8,128)(2,1)S(1)}, bf16[16,2048]{1,0:T(8,128)(2,1)S(1)}, u32[]{:S(2)}, u32[]{:S(2)}) collective-permute-start(bf16[16,2048]{1,0:T(8,128)(2,1)S(1)} %all_gather.12), channel_id=1, source_target_pairs={{0,18},{1,19},{2,16},{3,17},{4,22},{5,23},{6,20},{7,21},{8,26},{9,... | collective-permute-start | bytes 196616 | tf_op jit(solution)/shard_map/ppermute | solution.py:48
  37.9 15.0 %collective-permute-start.1 = (bf16[16,2048]{1,0:T(8,128)(2,1)S(1)}, bf16[16,2048]{1,0:T(8,128)(2,1)S(1)}, u32[]{:S(2)}, u32[]{:S(2)}) collective-permute-start(bf16[16,2048]{1,0:T(8,128)(2,1)S(1)} %all_gather.12), channel_id=1, source_target_pairs={{0,16},{1,17},{2,18},{3,19},{4,20},{5,21},{6,22},{7,23},{8,24},{9,... | collective-permute-start | bytes 196616 | tf_op jit(solution)/shard_map/ppermute | solution.py:48
  38.1 14.8 %collective-permute-start = (bf16[16,2048]{1,0:T(8,128)(2,1)S(1)}, bf16[16,2048]{1,0:T(8,128)(2,1)S(1)}, u32[]{:S(2)}, u32[]{:S(2)}) collective-permute-start(bf16[16,2048]{1,0:T(8,128)(2,1)S(1)} %all_gather.12), channel_id=1, source_target_pairs={{0,2},{1,3},{2,0},{3,1},{4,6},{5,7},{6,4},{7,5},{8,10},{9,11},{10,... | collective-permute-start | bytes 196616 | tf_op jit(solution)/shard_map/ppermute | solution.py:48
  53.3 7.1 %collective-permute-start.5 = (bf16[16,256]{1,0:T(8,128)(2,1)S(1)}, bf16[16,256]{1,0:T(8,128)(2,1)S(1)}, u32[]{:S(2)}, u32[]{:S(2)}) collective-permute-start(bf16[16,256]{1,0:T(8,128)(2,1)S(1)} %get-tuple-element.16), channel_id=1, source_target_pairs={{0,18},{1,19},{2,16},{3,17},{4,22},{5,23},{6,20},{7,21},{8,26},{9,... | collective-permute-start | bytes 24584 | tf_op jit(solution)/shard_map/ppermute | solution.py:48
  53.5 7.0 %collective-permute-start.4 = (bf16[16,256]{1,0:T(8,128)(2,1)S(1)}, bf16[16,256]{1,0:T(8,128)(2,1)S(1)}, u32[]{:S(2)}, u32[]{:S(2)}) collective-permute-start(bf16[16,256]{1,0:T(8,128)(2,1)S(1)} %get-tuple-element.17), channel_id=1, source_target_pairs={{0,16},{1,17},{2,18},{3,19},{4,20},{5,21},{6,22},{7,23},{8,24},{9,... | collective-permute-start | bytes 24584 | tf_op jit(solution)/shard_map/ppermute | solution.py:48
  53.6 6.9 %collective-permute-start.3 = (bf16[16,256]{1,0:T(8,128)(2,1)S(1)}, bf16[16,256]{1,0:T(8,128)(2,1)S(1)}, u32[]{:S(2)}, u32[]{:S(2)}) collective-permute-start(bf16[16,256]{1,0:T(8,128)(2,1)S(1)} %get-tuple-element.18), channel_id=1, source_target_pairs={{0,2},{1,3},{2,0},{3,1},{4,6},{5,7},{6,4},{7,5},{8,10},{9,11},{10,... | collective-permute-start | bytes 24584 | tf_op jit(solution)/shard_map/ppermute | solution.py:48
  64.9 27.5 %all-to-all-start.1 = ((bf16[64,2,2048]{2,1,0:T(2,128)(2,1)}), bf16[64,2,2048]{2,1,0:T(2,128)(2,1)S(1)}, u32[]{:S(2)}, u32[]{:S(2)}) async-start(bf16[64,2,2048]{2,1,0:T(2,128)(2,1)} %get-tuple-element.12), calls=%async_computation.1 | async-start | bytes 1048576 | tf_op jit(solution)/shard_map/all_to_all | solution.py:395
  92.7 0.8 copy-start.7
  95.0 36.3 %copy-start.1 = (bf16[2048,256]{1,0:T(8,128)(2,1)S(1)}, bf16[2048,256]{1,0:T(8,128)(2,1)}, u32[]{:S(2)}) copy-start(bf16[2048,256]{1,0:T(8,128)(2,1)} %gate_ref.1) | copy-start | bytes 3145732
  95.0 36.3 %copy-start.2 = (bf16[2048,256]{1,0:T(8,128)(2,1)S(1)}, bf16[2048,256]{1,0:T(8,128)(2,1)}, u32[]{:S(2)}) copy-start(bf16[2048,256]{1,0:T(8,128)(2,1)} %up_ref.1) | copy-start | bytes 3145732
  100.3 23.2 %all-to-all-start.2 = ((bf16[64,2,2048]{2,1,0:T(2,128)(2,1)}), bf16[64,2,2048]{2,1,0:T(2,128)(2,1)}, u32[]{:S(2)}, u32[]{:S(2)}) async-start(bf16[64,2,2048]{2,1,0:T(2,128)(2,1)} %reshape.83), calls=%async_computation.2 | async-start | bytes 1048576 | tf_op jit(solution)/shard_map/all_to_all | solution.py:416
  126.9 6.3 %collective-permute-start.6 = (f32[8,2048]{1,0:T(8,128)S(1)}, f32[8,2048]{1,0:T(8,128)S(1)}, u32[]{:S(2)}, u32[]{:S(2)}) collective-permute-start(f32[8,2048]{1,0:T(8,128)S(1)} %constant_dynamic-slice_fusion.1), channel_id=1, source_target_pairs={{0,1},{1,0},{2,3},{3,2},{4,5},{5,4},{6,7},{7,6},{8,9},{9,8},{10,11... | collective-permute-start | bytes 196616 | tf_op jit(solution)/shard_map/ppermute | solution.py:61
  131.4 1.2 copy-start.3

commit v2 on v1

--- a/solution.py
+++ b/solution.py
@@ -1,3 +1,5 @@
+import math
+
 import jax
 import jax.numpy as jnp
 from jax import lax
@@ -65,21 +67,12 @@
     return values * lax.rsqrt(jnp.mean(values * values, axis=-1, keepdims=True) + norm_eps)
 
 
-def swiglu(flat_rows, gate_w, up_w, down_w):
-    gate_part = jnp.dot(flat_rows, gate_w, preferred_element_type=jnp.float32)
-    up_part = jnp.dot(flat_rows, up_w, preferred_element_type=jnp.float32)
-    inner_rows = (jax.nn.silu(gate_part) * up_part).astype(jnp.bfloat16)
-    return jnp.dot(inner_rows, down_w, preferred_element_type=jnp.float32).astype(jnp.bfloat16)
-
-
 def attention_kernel(
     lengths_ref,
     nope_ref,
     rope_ref,
     latent_ref,
     key_ref,
-    cosine_ref,
-    sine_ref,
     absorb_ref,
     cache_ref,
     cache_rope_ref,
@@ -112,14 +105,22 @@
             wide.astype(jnp.bfloat16), absorb_ref[...], preferred_element_type=jnp.float32
         )
         query_ref[...] = queries.reshape(seq_count, heads, latent).astype(jnp.bfloat16)
-        cosine = cosine_ref[...][:, None, :]
-        sine = sine_ref[...][:, None, :]
-        query_pe_ref[...] = turned(rope_ref[...].astype(jnp.float32), cosine, sine).astype(
-            jnp.bfloat16
-        )
+        row = lax.broadcasted_iota(jnp.int32, (seq_count, rope), 0)
+        column = lax.broadcasted_iota(jnp.int32, (seq_count, rope), 1)
+        position = jnp.zeros((seq_count, rope), jnp.int32)
+        for n in range(seq_count):
+            position = jnp.where(row == n, lengths_ref[n], position)
+        exponent = (column % half).astype(jnp.float32) * (-2.0 / rope * math.log(rope_theta))
+        angles = position.astype(jnp.float32) * jnp.exp(exponent)
+        cosine = jnp.cos(angles)
+        sine = jnp.sin(angles)
+        sine = jnp.where(column < half, -sine, sine)
+        query_pe_ref[...] = turned(
+            rope_ref[...].astype(jnp.float32), cosine[:, None, :], sine[:, None, :]
+        ).astype(jnp.bfloat16)
         latent_new = normalize(latent_ref[...].astype(jnp.float32)).astype(jnp.bfloat16)
         latent_new_ref[...] = latent_new.astype(jnp.float32)[:, None, :]
-        key_new = turned(key_ref[...].astype(jnp.float32), cosine_ref[...], sine_ref[...])
+        key_new = turned(key_ref[...].astype(jnp.float32), cosine, sine)
         key_new_ref[...] = key_new.astype(jnp.bfloat16).astype(jnp.float32)[:, None, :]
 
     for place in range(cache_ref.shape[0]):
@@ -157,12 +158,6 @@
     rope = query_rope.shape[-1]
     latent = cache_latent.shape[-1]
     context = cache_latent.shape[1]
-    half = rope // 2
-    inverse = rope_theta ** (-jnp.arange(half, dtype=jnp.float32) * 2.0 / rope)
-    angles = lengths.astype(jnp.float32)[:, None] * jnp.concatenate([inverse, inverse])[None, :]
-    sign = jnp.where(jnp.arange(rope) < half, -1.0, 1.0)
-    cosine = jnp.cos(angles)
-    sine = jnp.sin(angles) * sign[None, :]
     absorb = absorb_key.transpose(1, 2, 0).reshape(heads * nope, latent)
     rope_turned = cache_rope.transpose(0, 2, 1)
     whole = lambda *shape: pl.BlockSpec(shape, lambda step, lengths: (0,) * len(shape))
@@ -175,8 +170,6 @@
                 whole(seq_count, heads, nope),
                 whole(seq_count, heads, rope),
                 whole(seq_count, latent),
-                whole(seq_count, rope),
-                whole(seq_count, rope),
                 whole(seq_count, rope),
                 whole(heads * nope, latent),
                 pl.BlockSpec((SEQ_STEP, context, latent), lambda step, lengths: (step, 0, 0)),
@@ -199,7 +192,7 @@
         ),
         name="attended",
     )(
-        lengths, query_nope, query_rope, new_latent, new_rope, cosine, sine, absorb, cache_latent, rope_turned
+        lengths, query_nope, query_rope, new_latent, new_rope, absorb, cache_latent, rope_turned
     )
 
 
@@ -227,7 +220,8 @@
 def spread_kernel(
     place_ref,
     pieces_ref,
-    hidden_ref,
+    own_hidden_ref,
+    other_hidden_ref,
     gain_mix_ref,
     gain_in_ref,
     routes_ref,
@@ -237,7 +231,8 @@
     taken_ref,
 ):
     core, block_i, block_j = place_ref[0], place_ref[1], place_ref[2]
-    rows, _ = hidden_ref.shape
+    half = own_hidden_ref.shape[0]
+    rows = 2 * half
     piece = pieces_ref.shape[-1]
     run = piece // 4
     chunks = []
@@ -264,14 +259,22 @@
     mixed = jnp.concatenate(
         [placed[n * rows : (n + 1) * rows] for n in range(len(chunks))], axis=-1
     )
+    own_hidden = own_hidden_ref[...].astype(jnp.float32)
+    other_hidden = other_hidden_ref[...].astype(jnp.float32)
+    hidden = jnp.concatenate(
+        [
+            jnp.where(core == 0, own_hidden, other_hidden),
+            jnp.where(core == 0, other_hidden, own_hidden),
+        ],
+        axis=0,
+    )
     after_mix = (
-        hidden_ref[...].astype(jnp.float32)
+        hidden
         + gain_mix_ref[...].astype(jnp.float32)[None] * normalize(mixed)
     ).astype(jnp.bfloat16)
     after_wide = after_mix.astype(jnp.float32)
     ffn_in = (normalize(after_wide) * gain_in_ref[...].astype(jnp.float32)[None]).astype(jnp.bfloat16)
     ffn_ref[...] = ffn_in
-    half = rows // 2
     mix_ref[...] = jnp.where(core == 0, after_wide[:half], after_wide[half:]).astype(jnp.bfloat16)
     slots = taken_ref.shape[0]
     slot = lax.broadcasted_iota(jnp.int32, (slots, rows), 0)
@@ -292,12 +295,12 @@
     outgoing_ref[...] = outgoing.reshape(outgoing_ref.shape)
 
 
-def spread(place, pieces, chip_hidden, gain_mix, gain_in, routes, slots):
-    rows, width = chip_hidden.shape
+def spread(place, pieces, own_hidden, other_hidden, gain_mix, gain_in, routes, slots):
+    rows, width = 2 * own_hidden.shape[0], own_hidden.shape[1]
     return pl.pallas_call(
         spread_kernel,
         in_specs=[pl.BlockSpec(memory_space=pltpu.SMEM)]
-        + [pl.BlockSpec(memory_space=pltpu.VMEM)] * 5,
+        + [pl.BlockSpec(memory_space=pltpu.VMEM)] * 6,
         out_specs=[pl.BlockSpec(memory_space=pltpu.VMEM)] * 4,
         out_shape=[
             jax.ShapeDtypeStruct((slots // 2, 2, width), jnp.bfloat16),
@@ -307,17 +310,16 @@
         ],
         compiler_params=pltpu.CompilerParams(vmem_limit_bytes=8 << 20),
         name="spread",
-    )(place, pieces, chip_hidden, gain_mix, gain_in, routes.T)
+    )(place, pieces, own_hidden, other_hidden, gain_mix, gain_in, routes.T)
 
 
 def experts_kernel(rows_ref, gate_ref, up_ref, down_ref, out_ref):
-    rows = rows_ref[...]
+    rows = rows_ref[...].reshape(-1, rows_ref.shape[-1])
     gate_part = jnp.dot(rows, gate_ref[...], preferred_element_type=jnp.float32)
     up_part = jnp.dot(rows, up_ref[...], preferred_element_type=jnp.float32)
     inner = (gate_part / (1.0 + jnp.exp(-gate_part)) * up_part).astype(jnp.bfloat16)
-    out_ref[...] = jnp.dot(inner, down_ref[...], preferred_element_type=jnp.float32).astype(
-        out_ref.dtype
-    )
+    out = jnp.dot(inner, down_ref[...], preferred_element_type=jnp.float32)
+    out_ref[...] = out.astype(out_ref.dtype).reshape(out_ref.shape)
 
 
 def expert_rows(rows, gate_w, up_w, down_w):
@@ -325,8 +327,84 @@
         experts_kernel,
         in_specs=[pl.BlockSpec(memory_space=pltpu.VMEM)] * 4,
         out_specs=pl.BlockSpec(memory_space=pltpu.VMEM),
-        out_shape=jax.ShapeDtypeStruct((rows.shape[0], down_w.shape[1]), jnp.bfloat16),
+        out_shape=jax.ShapeDtypeStruct(rows.shape, jnp.bfloat16),
         compiler_params=pltpu.CompilerParams(vmem_limit_bytes=10 << 20),
+    )(rows, gate_w, up_w, down_w)
+
+
+def gathered_kernel(place_ref, weights_ref, returned_ref, shared_ref, kept_ref, given_ref):
+    core = place_ref[0]
+    rows = weights_ref.shape[0] // 2
+    half = rows // 2
+    returned = returned_ref[...].reshape(-1, returned_ref.shape[-1])
+    both = jnp.dot(weights_ref[...], returned, preferred_element_type=jnp.float32)
+    routed = both[:rows] + both[rows:]
+    first, second = routed[:half], routed[half:]
+    shared = shared_ref[...].astype(jnp.float32)
+    kept_ref[...] = jnp.where(core == 0, first, second) + shared
+    given_ref[...] = jnp.where(core == 0, second, first)
+
+
+def gathered(place, weights, returned, shared):
+    shape = jax.ShapeDtypeStruct(shared.shape, jnp.float32)
+    return pl.pallas_call(
+        gathered_kernel,
+        in_specs=[pl.BlockSpec(memory_space=pltpu.SMEM)]
+        + [pl.BlockSpec(memory_space=pltpu.VMEM)] * 3,
+        out_specs=[pl.BlockSpec(memory_space=pltpu.VMEM)] * 2,
+        out_shape=[shape, shape],
+        compiler_params=pltpu.CompilerParams(vmem_limit_bytes=8 << 20),
+        name="gathered",
+    )(place, weights, returned, shared)
+
+
+def routed_kernel(
+    rows_hbm,
+    gate_hbm,
+    up_hbm,
+    down_hbm,
+    out_ref,
+    rows_ref,
+    gate_ref,
+    up_ref,
+    down_ref,
+    arrived,
+):
+    moves = [
+        pltpu.make_async_copy(source, target, arrived.at[n])
+        for n, (source, target) in enumerate(
+            (
+                (rows_hbm, rows_ref),
+                (gate_hbm, gate_ref),
+                (up_hbm, up_ref),
+                (down_hbm, down_ref),
+            )
+        )
+    ]
+    for move in moves:
+        move.start()
+    moves[0].wait()
+    rows = rows_ref[...].reshape(-1, rows_ref.shape[-1])
+    moves[1].wait()
+    gate_part = jnp.dot(rows, gate_ref[...], preferred_element_type=jnp.float32)
+    moves[2].wait()
+    up_part = jnp.dot(rows, up_ref[...], preferred_element_type=jnp.float32)
+    inner = (gate_part / (1.0 + jnp.exp(-gate_part)) * up_part).astype(jnp.bfloat16)
+    moves[3].wait()
+    out = jnp.dot(inner, down_ref[...], preferred_element_type=jnp.float32)
+    out_ref[...] = out.astype(out_ref.dtype).reshape(out_ref.shape)
+
+
+def routed_rows(rows, gate_w, up_w, down_w):
+    return pl.pallas_call(
+        routed_kernel,
+        in_specs=[pl.BlockSpec(memory_space=pltpu.HBM)] * 4,
+        out_specs=pl.BlockSpec(memory_space=pltpu.VMEM),
+        out_shape=jax.ShapeDtypeStruct(rows.shape, jnp.bfloat16),
+        scratch_shapes=[pltpu.VMEM(w.shape, w.dtype) for w in (rows, gate_w, up_w, down_w)]
+        + [pltpu.SemaphoreType.DMA((4,))],
+        compiler_params=pltpu.CompilerParams(vmem_limit_bytes=64300 << 10),
+        name="routed",
     )(rows, gate_w, up_w, down_w)
 
 
@@ -354,11 +432,11 @@
     shared_down,
     gain_ffn_out,
 ):
-    seq_count, width = hidden_in.shape
+    seq_count, _ = hidden_in.shape
     core = lax.axis_index("tp")
     own_start = core * seq_count
     slab = sent_to_all(out_proj.T, PLACES).reshape(-1, out_proj.shape[0])
-    chip_hidden = lax.all_gather(hidden_in, "tp", axis=0, tiled=True)
+    other_hidden = from_other_core(hidden_in)
     heads_out = attention(
         query_nope,
         query_rope,
@@ -383,6 +461,7 @@
     )
     pieces = lax.all_gather(pieces, "tp", axis=0)
     place = jnp.stack([core, lax.axis_index("ep_0") % 2, lax.axis_index("ep_1") % 2])
+    place = place.astype(jnp.int32)
     experts_total = router.shape[1]
     group_rows, top_count = routes.shape
     ep_count = lax.axis_size(EP)
@@ -390,7 +469,7 @@
     slots = ep_count * capacity
     slot_expert = lax.iota(jnp.int32, slots) // capacity * 2 + core
     outgoing, ffn_in, own_mix, taken = spread(
-        place.astype(jnp.int32), pieces, chip_hidden, gain_mix, gain_ffn_in, routes, slots
+        place, pieces, hidden_in, other_hidden, gain_mix, gain_ffn_in, routes, slots
     )
     received = lax.all_to_all(
         outgoing, EP, split_axis=0, concat_axis=0, tiled=True
@@ -410,21 +489,11 @@
     weights_low = (slot_weights - weights_high.astype(jnp.float32)).astype(jnp.bfloat16)
     own_ffn = lax.dynamic_slice_in_dim(ffn_in, own_start, seq_count, 0)
     shared = expert_rows(own_ffn, shared_gate, shared_up, shared_down)
-    outputs = swiglu(
-        received.reshape(slots, width), expert_gate[0], expert_up[0], expert_down[0]
-    )
-    returned = lax.all_to_all(
-        outputs.reshape(ep_count, capacity, width), EP, split_axis=0, concat_axis=0, tiled=True
-    ).reshape(slots, width)
-    both = jnp.dot(
-        jnp.concatenate([weights_high, weights_low], axis=0),
-        returned,
-        preferred_element_type=jnp.float32,
-    )
-    routed = both[:group_rows] + both[group_rows:]
-    kept = lax.dynamic_slice_in_dim(routed, own_start, seq_count, 0)
-    given = lax.dynamic_slice_in_dim(routed, seq_count - own_start, seq_count, 0)
-    combined = kept + from_other_core(given) + shared.astype(jnp.float32)
+    outputs = routed_rows(received, expert_gate[0], expert_up[0], expert_down[0])
+    returned = lax.all_to_all(outputs, EP, split_axis=0, concat_axis=0, tiled=True)
+    weights = jnp.concatenate([weights_high, weights_low], axis=0)
+    kept, given = gathered(place, weights, returned, shared)
+    combined = kept + from_other_core(given)
     return (
         own_mix.astype(jnp.float32) + gain_ffn_out.astype(jnp.float32) * normalize(combined)
     ).astype(jnp.bfloat16)

time: 135 us -> 127 us (0.941)
  matrix products: 8.73 us -> 1.82 us
  Pallas kernels: 9.78 us -> 13.9 us
  local copies, waits for them, and re-layouts: 8.83 us -> 5.84 us
  other arithmetic: 2.8 us -> 1.26 us
    dot_general x3 -> x0, matrix products: 5.88 us -> none  [the longest x1 3.1 us: swiglu(): jnp.dot(inner_rows, down_w, preferred_element_type=jnp.float32)]
    reshape x3 -> x0, local copies, waits for them, and re-layouts: 4.43 us -> none  [the longest x1 2.19 us: local(): outputs.reshape(ep_count, capacity, width)]
    all_gather x1 -> x0, blocking collectives: 4.37 us -> none  [local(): chip_hidden = lax.all_gather(hidden_in, 'tp', axis=0, tiled=True)]
    pallas_call x0 -> x2, Pallas kernels: none -> 4.13 us  [the longest x1 3.39 us: routed_rows(): pl.pallas_call(routed_kernel, in_specs=[pl.BlockSpec(memory_space=pltpu.H...]
    all_gather x1, blocking collectives: 2.34 us -> 6.01 us  [local(): pieces = lax.all_gather(pieces, 'tp', axis=0)]
    all_to_all x1, waiting for transfers between devices: 13.1 us -> 10.1 us  [local(): lax.all_to_all(outputs, EP, split_axis=0, concat_axis=0, tiled=True)]
    unnamed x22 -> x20, local copies, waits for them, and re-layouts: 2.06 us -> 3.74 us
    ppermute x1 -> x2, starting transfers between devices: 4.44 us -> 5.62 us  [from_other_core(): return lax.ppermute(array, 'tp', [(0, 1), (1, 0)])]
  transfers between devices with their start and end apart: 10 -> 11, of which waited for: 4 -> 7; matrix products, arithmetic and copies ran while one was open for 3% -> 2% of each run, Pallas kernels for 6% -> 6%
where the time goes in v2:
time: 127 us; the launch traced here: 126 us
  starting transfers between devices  49.7 us (39%)
  waiting for transfers between devices  40.5 us (32%)
  Pallas kernels  13.9 us (11%)
  blocking collectives  13 us (10%)
  local copies, waits for them, and re-layouts  5.84 us (5%)
  matrix products  1.82 us (1%)
    all_to_all x1, starting transfers between devices, exchanged(): lax.all_to_all(blocks, EP_TP, 0, 0, axis_index_groups=groups, tiled=True)  19.2 us
    all_to_all x1, waiting for transfers between devices, local(): lax.all_to_all(outgoing, EP, split_axis=0, concat_axis=0, tiled=True)  16.3 us
    ppermute x6, waiting for transfers between devices, from_partner(): return lax.ppermute(array, EP_TP, partners(flip // 2, flip % 2))  13.2 us
    all_to_all x1, starting transfers between devices, local(): lax.all_to_all(outgoing, EP, split_axis=0, concat_axis=0, tiled=True)  11.2 us
    all_to_all x1, waiting for transfers between devices, local(): lax.all_to_all(outputs, EP, split_axis=0, concat_axis=0, tiled=True)  10.1 us
    all_to_all x1, starting transfers between devices, local(): lax.all_to_all(outputs, EP, split_axis=0, concat_axis=0, tiled=True)  8.35 us
    pallas_call x1, Pallas kernels, attended(): pl.pallas_call(attention_kernel, grid_spec=pltpu.PrefetchScalarGridSpec(n...  7.08 us
    all_gather x1, blocking collectives, local(): chip_heads = lax.all_gather(heads_out, 'tp', axis=0, tiled=True)  6.98 us
  transfers between devices with their start and end apart: 11, of which 7 were waited for; matrix products, arithmetic and copies ran while one was open for 2% of the time, Pallas kernels for 6%

profile of v2, /device:TPU:513, one launch (start us, length us, event | category | flops | bytes accessed | tf_op | source)
XLA Modules:
  0.0 126.1 jit_solution(8673520681319648794)
XLA Ops:
  0.0 0.0 copy-start
  0.0 2.0 %broadcast_in_dim.20 = bf16[16,16,2048]{2,1,0:T(8,128)(2,1)} broadcast(bf16[16,2048]{1,0:T(8,128)(2,1)} %bitcast.42), dimensions={1,2} | broadcast | bytes 1114112 | tf_op jit(solution)/shard_map/broadcast_in_dim | solution.py:59
  2.0 0.0 copy-start.5
  2.0 19.2 %all-to-all-start = ((bf16[16,16,2048]{2,1,0:T(8,128)(2,1)}), bf16[16,16,2048]{2,1,0:T(8,128)(2,1)S(1)}, u32[]{:S(2)}, u32[]{:S(2)}) async-start(bf16[16,16,2048]{2,1,0:T(8,128)(2,1)} %broadcast_in_dim.20), calls=%async_computation | async-start | bytes 2097152 | tf_op jit(solution)/shard_map/all_to_all | solution.py:54
  21.2 0.0 copy-start.4
  21.2 0.0 copy-start.6
  21.2 0.0 copy-start.7
  21.3 7.1 %attended.1 = bf16[8,16,256]{2,1,0:T(8,128)(2,1)} custom-call(s32[8]{0:T(128)} %lengths_ref.1, bf16[8,16,64]{2,1,0:T(8,128)(2,1)} %nope_ref.1, bf16[8,16,32]{2,1,0:T(8,128)(2,1)} %rope_ref.1, bf16[8,256]{1,0:T(8,128)(2,1)} %latent_ref.1, bf16[8,32]{1,0:T(8,128)(2,1)} %key_ref.1, bf16[1024,256]{1,0:T(8,128)(2,1)} %bitcast.40, ...), custom_call_target="tpu_custom_call" | custom-call | flops 268435456 | bytes 4718592 | tf_op jit(solution)/shard_map/attended/pallas_call | solution.py:164
  28.3 0.0 copy-done
  28.3 1.2 fusion
  29.5 7.0 %all_gather.9 = bf16[16,2048]{1,0:T(8,128)(2,1)S(1)} all-gather(bf16[8,2048]{1,0:T(8,128)(2,1)S(1)} %fusion), channel_id=1, replica_groups=mesh['grp'=2,'ep_0'=8,'ep_1'=8,'tp'=2] {'tp'}, dimensions={0}, use_global_device_ids=true | all-gather | bytes 98304 | tf_op jit(solution)/shard_map/all_gather | solution.py:451
  36.5 0.0 collective-permute-start.2
  36.5 0.1 collective-permute-start.1
  36.6 2.5 %collective-permute-start = (bf16[16,2048]{1,0:T(8,128)(2,1)S(1)}, bf16[16,2048]{1,0:T(8,128)(2,1)S(1)}, u32[]{:S(2)}, u32[]{:S(2)}) collective-permute-start(bf16[16,2048]{1,0:T(8,128)(2,1)S(1)} %all_gather.9), channel_id=1, source_target_pairs={{0,2},{1,3},{2,0},{3,1},{4,6},{5,7},{6,4},{7,5},{8,10},{9,11},{10,... | collective-permute-start | bytes 196616 | tf_op jit(solution)/shard_map/ppermute | solution.py:50
  39.1 0.0 copy-done.5
  39.1 1.3 %collective-permute-start.6 = (bf16[8,2048]{1,0:T(8,128)(2,1)S(1)}, bf16[8,2048]{1,0:T(8,128)(2,1)S(1)}, u32[]{:S(2)}, u32[]{:S(2)}) collective-permute-start(bf16[8,2048]{1,0:T(8,128)(2,1)S(1)} %copy-done.5), channel_id=1, source_target_pairs={{0,1},{1,0},{2,3},{3,2},{4,5},{5,4},{6,7},{7,6},{8,9},{9,8},{10,11... | collective-permute-start | bytes 98312 | tf_op jit(solution)/shard_map/ppermute | solution.py:63
  40.4 9.2 %collective-permute-done.2 = bf16[16,2048]{1,0:T(8,128)(2,1)S(1)} collective-permute-done((bf16[16,2048]{1,0:T(8,128)(2,1)S(1)}, bf16[16,2048]{1,0:T(8,128)(2,1)S(1)}, u32[]{:S(2)}, u32[]{:S(2)}) %collective-permute-start.2) | collective-permute-done | bytes 65568 | tf_op jit(solution)/shard_map/ppermute | solution.py:50
  49.6 3.0 %collective-permute-done.1 = bf16[16,2048]{1,0:T(8,128)(2,1)S(1)} collective-permute-done((bf16[16,2048]{1,0:T(8,128)(2,1)S(1)}, bf16[16,2048]{1,0:T(8,128)(2,1)S(1)}, u32[]{:S(2)}, u32[]{:S(2)}) %collective-permute-start.1) | collective-permute-done | bytes 65568 | tf_op jit(solution)/shard_map/ppermute | solution.py:50
  52.7 0.0 collective-permute-done
  52.7 0.0 all-to-all-done
  52.7 0.4 convolution_convert_fusion
  53.1 0.1 collective-permute-start.5
  53.3 0.2 collective-permute-start.4
  53.5 2.4 %collective-permute-start.3 = (bf16[16,256]{1,0:T(8,128)(2,1)S(1)}, bf16[16,256]{1,0:T(8,128)(2,1)S(1)}, u32[]{:S(2)}, u32[]{:S(2)}) collective-permute-start(bf16[16,256]{1,0:T(8,128)(2,1)S(1)} %get-tuple-element.24), channel_id=1, source_target_pairs={{0,2},{1,3},{2,0},{3,1},{4,6},{5,7},{6,4},{7,5},{8,10},{9,11},{10,... | collective-permute-start | bytes 24584 | tf_op jit(solution)/shard_map/ppermute | solution.py:50
  55.9 0.1 pad_add_fusion.place_ref
  56.0 0.7 collective-permute-done.5
  56.7 0.0 collective-permute-done.4
  56.7 0.3 collective-permute-done.3
  57.0 6.0 %all-gather = bf16[8,16,256]{2,1,0:T(8,128)(2,1)S(1)} all-gather(bf16[4,16,256]{2,1,0:T(8,128)(2,1)S(1)} %pad_maximum_fusion), channel_id=2, replica_groups=mesh['grp'=2,'ep_0'=8,'ep_1'=8,'tp'=2] {'tp'}, dimensions={0}, use_global_device_ids=true | all-gather | bytes 98304 | tf_op jit(solution)/shard_map/all_gather | solution.py:462
  63.0 0.0 collective-permute-done.6.other_hidden_ref
  63.0 0.0 copy-done.4
  63.0 0.0 copy-done.6
  63.0 0.0 copy-done.7
  63.0 2.1 %spread.1 = (bf16[64,2,2048]{2,1,0:T(2,128)(2,1)}, bf16[16,2048]{1,0:T(8,128)(2,1)S(1)}, bf16[8,2048]{1,0:T(8,128)(2,1)S(1)}, bf16[128,16]{1,0:T(8,128)(2,1)S(1)}) custom-call(s32[3]{0:T(128)S(1)} %pad_add_fusion.place_ref, bf16[2,4,16,256]{3,2,1,0:T(8,128)(2,1)S(1)} %bitcast.34, bf16[8,2048]{1,0:T(8,128)(2,1)S(1)} %copy-done.5, ...), custom_call_target="tpu_custom_call" | custom-call | tf_op jit(solution)/shard_map/spread/pallas_call | solution.py:300
  65.1 11.2 %all-to-all-start.1 = ((bf16[64,2,2048]{2,1,0:T(2,128)(2,1)}), bf16[64,2,2048]{2,1,0:T(2,128)(2,1)}, u32[]{:S(2)}, u32[]{:S(2)}) async-start(bf16[64,2,2048]{2,1,0:T(2,128)(2,1)} %get-tuple-element.14), calls=%async_computation.1 | async-start | bytes 1048576 | tf_op jit(solution)/shard_map/all_to_all | solution.py:474
  76.2 16.3 %all-to-all-done.1.rows_hbm = bf16[64,2,2048]{2,1,0:T(2,128)(2,1)} async-done(((bf16[64,2,2048]{2,1,0:T(2,128)(2,1)}), bf16[64,2,2048]{2,1,0:T(2,128)(2,1)}, u32[]{:S(2)}, u32[]{:S(2)}) %all-to-all-start.1) | async-done | bytes 524320 | tf_op jit(solution)/shard_map/all_to_all | solution.py:474
  92.5 0.0 copy-start.9
  92.5 3.4 %routed.1 = bf16[64,2,2048]{2,1,0:T(2,128)(2,1)} custom-call(bf16[64,2,2048]{2,1,0:T(2,128)(2,1)} %all-to-all-done.1.rows_hbm, bf16[2048,256]{1,0:T(8,128)(2,1)} %bitcast.37, bf16[2048,256]{1,0:T(8,128)(2,1)} %bitcast.38, bf16[256,2048]{1,0:T(8,128)(2,1)} %bitcast.39), custom_call_target="tpu_custom_call" | custom-call | tf_op jit(solution)/shard_map/routed/pallas_call | solution.py:399
  95.9 0.0 copy-start.8
  95.9 8.3 %all-to-all-start.2 = ((bf16[64,2,2048]{2,1,0:T(2,128)(2,1)}), bf16[64,2,2048]{2,1,0:T(2,128)(2,1)S(1)}, u32[]{:S(2)}, u32[]{:S(2)}) async-start(bf16[64,2,2048]{2,1,0:T(2,128)(2,1)} %routed.1), calls=%async_computation.2 | async-start | bytes 1048576 | tf_op jit(solution)/shard_map/all_to_all | solution.py:493
  104.3 0.1 copy.33
  104.4 0.0 copy-start.1
  104.4 1.2 copy-done.1
  105.6 0.0 copy-start.2
  105.6 1.2 copy-done.2
  106.8 0.0 copy-start.3
  106.8 1.2 copy-done.3
  108.1 0.6 shard_map.208.shared_ref
  108.7 0.0 copy-done.8
  108.7 0.2 fusion.3
  108.9 0.2 select_reduce_fusion
  109.1 0.1 select_reduce_fusion.2
  109.2 10.1 %all-to-all-done.2.returned_ref = bf16[64,2,2048]{2,1,0:T(2,128)(2,1)S(1)} async-done(((bf16[64,2,2048]{2,1,0:T(2,128)(2,1)}), bf16[64,2,2048]{2,1,0:T(2,128)(2,1)S(1)}, u32[]{:S(2)}, u32[]{:S(2)}) %all-to-all-start.2) | async-done | bytes 524320 | tf_op jit(solution)/shard_map/all_to_all | solution.py:493
  119.3 0.7 gathered.1
  120.0 4.3 %collective-permute-start.7 = (f32[8,2048]{1,0:T(8,128)S(1)}, f32[8,2048]{1,0:T(8,128)S(1)}, u32[]{:S(2)}, u32[]{:S(2)}) collective-permute-start(f32[8,2048]{1,0:T(8,128)S(1)} %get-tuple-element.16), channel_id=1, source_target_pairs={{0,1},{1,0},{2,3},{3,2},{4,5},{5,4},{6,7},{7,6},{8,9},{9,8},{10,11... | collective-permute-start | bytes 196616 | tf_op jit(solution)/shard_map/ppermute | solution.py:63
  124.4 0.0 copy-done.9
  124.4 0.9 collective-permute-done.7
  125.3 0.1 multiply_reduce_fusion
  125.4 0.7 add_convert_fusion
  (9 shorter events, 0.1 us)
Async XLA Ops:
  0.0 28.3 %copy-start = (bf16[256,16,128]{2,1,0:T(8,128)(2,1)S(1)}, bf16[256,16,128]{2,1,0:T(8,128)(2,1)}, u32[]{:S(2)}) copy-start(bf16[256,16,128]{2,1,0:T(8,128)(2,1)} %param.31) | copy-start | bytes 3145732
  2.0 37.1 %copy-start.5 = (bf16[8,2048]{1,0:T(8,128)(2,1)S(1)}, bf16[8,2048]{1,0:T(8,128)(2,1)}, u32[]{:S(2)}) copy-start(bf16[8,2048]{1,0:T(8,128)(2,1)} %own_hidden_ref.1) | copy-start | bytes 98308
  2.0 50.7 %all-to-all-start = ((bf16[16,16,2048]{2,1,0:T(8,128)(2,1)}), bf16[16,16,2048]{2,1,0:T(8,128)(2,1)S(1)}, u32[]{:S(2)}, u32[]{:S(2)}) async-start(bf16[16,16,2048]{2,1,0:T(8,128)(2,1)} %broadcast_in_dim.20), calls=%async_computation | async-start | bytes 2097152 | tf_op jit(solution)/shard_map/all_to_all | solution.py:54
  21.2 41.7 %copy-start.4 = (s32[16,6]{0,1:T(8,128)S(1)}, s32[16,6]{0,1:T(8,128)}, u32[]{:S(2)}) copy-start(s32[16,6]{0,1:T(8,128)} %param.36) | copy-start | bytes 1156
  21.2 41.7 %copy-start.6 = (bf16[2048]{0:T(1024)(128)(2,1)S(1)}, bf16[2048]{0:T(1024)(128)(2,1)}, u32[]{:S(2)}) copy-start(bf16[2048]{0:T(1024)(128)(2,1)} %gain_mix_ref.1) | copy-start | bytes 12292
  21.2 41.7 %copy-start.7 = (bf16[2048]{0:T(1024)(128)(2,1)S(1)}, bf16[2048]{0:T(1024)(128)(2,1)}, u32[]{:S(2)}) copy-start(bf16[2048]{0:T(1024)(128)(2,1)} %gain_in_ref.1) | copy-start | bytes 12292
  36.5 13.1 %collective-permute-start.2 = (bf16[16,2048]{1,0:T(8,128)(2,1)S(1)}, bf16[16,2048]{1,0:T(8,128)(2,1)S(1)}, u32[]{:S(2)}, u32[]{:S(2)}) collective-permute-start(bf16[16,2048]{1,0:T(8,128)(2,1)S(1)} %all_gather.9), channel_id=1, source_target_pairs={{0,18},{1,19},{2,16},{3,17},{4,22},{5,23},{6,20},{7,21},{8,26},{9,... | collective-permute-start | bytes 196616 | tf_op jit(solution)/shard_map/ppermute | solution.py:50
  36.5 16.2 %collective-permute-start.1 = (bf16[16,2048]{1,0:T(8,128)(2,1)S(1)}, bf16[16,2048]{1,0:T(8,128)(2,1)S(1)}, u32[]{:S(2)}, u32[]{:S(2)}) collective-permute-start(bf16[16,2048]{1,0:T(8,128)(2,1)S(1)} %all_gather.9), channel_id=1, source_target_pairs={{0,16},{1,17},{2,18},{3,19},{4,20},{5,21},{6,22},{7,23},{8,24},{9,... | collective-permute-start | bytes 196616 | tf_op jit(solution)/shard_map/ppermute | solution.py:50
  36.6 16.0 %collective-permute-start = (bf16[16,2048]{1,0:T(8,128)(2,1)S(1)}, bf16[16,2048]{1,0:T(8,128)(2,1)S(1)}, u32[]{:S(2)}, u32[]{:S(2)}) collective-permute-start(bf16[16,2048]{1,0:T(8,128)(2,1)S(1)} %all_gather.9), channel_id=1, source_target_pairs={{0,2},{1,3},{2,0},{3,1},{4,6},{5,7},{6,4},{7,5},{8,10},{9,11},{10,... | collective-permute-start | bytes 196616 | tf_op jit(solution)/shard_map/ppermute | solution.py:50
  39.1 23.8 %collective-permute-start.6 = (bf16[8,2048]{1,0:T(8,128)(2,1)S(1)}, bf16[8,2048]{1,0:T(8,128)(2,1)S(1)}, u32[]{:S(2)}, u32[]{:S(2)}) collective-permute-start(bf16[8,2048]{1,0:T(8,128)(2,1)S(1)} %copy-done.5), channel_id=1, source_target_pairs={{0,1},{1,0},{2,3},{3,2},{4,5},{5,4},{6,7},{7,6},{8,9},{9,8},{10,11... | collective-permute-start | bytes 98312 | tf_op jit(solution)/shard_map/ppermute | solution.py:63
  53.1 3.5 %collective-permute-start.5 = (bf16[16,256]{1,0:T(8,128)(2,1)S(1)}, bf16[16,256]{1,0:T(8,128)(2,1)S(1)}, u32[]{:S(2)}, u32[]{:S(2)}) collective-permute-start(bf16[16,256]{1,0:T(8,128)(2,1)S(1)} %get-tuple-element.22), channel_id=1, source_target_pairs={{0,18},{1,19},{2,16},{3,17},{4,22},{5,23},{6,20},{7,21},{8,26},{9,... | collective-permute-start | bytes 24584 | tf_op jit(solution)/shard_map/ppermute | solution.py:50
  53.3 3.4 %collective-permute-start.4 = (bf16[16,256]{1,0:T(8,128)(2,1)S(1)}, bf16[16,256]{1,0:T(8,128)(2,1)S(1)}, u32[]{:S(2)}, u32[]{:S(2)}) collective-permute-start(bf16[16,256]{1,0:T(8,128)(2,1)S(1)} %get-tuple-element.23), channel_id=1, source_target_pairs={{0,16},{1,17},{2,18},{3,19},{4,20},{5,21},{6,22},{7,23},{8,24},{9,... | collective-permute-start | bytes 24584 | tf_op jit(solution)/shard_map/ppermute | solution.py:50
  53.5 3.5 %collective-permute-start.3 = (bf16[16,256]{1,0:T(8,128)(2,1)S(1)}, bf16[16,256]{1,0:T(8,128)(2,1)S(1)}, u32[]{:S(2)}, u32[]{:S(2)}) collective-permute-start(bf16[16,256]{1,0:T(8,128)(2,1)S(1)} %get-tuple-element.24), channel_id=1, source_target_pairs={{0,2},{1,3},{2,0},{3,1},{4,6},{5,7},{6,4},{7,5},{8,10},{9,11},{10,... | collective-permute-start | bytes 24584 | tf_op jit(solution)/shard_map/ppermute | solution.py:50
  65.1 27.4 %all-to-all-start.1 = ((bf16[64,2,2048]{2,1,0:T(2,128)(2,1)}), bf16[64,2,2048]{2,1,0:T(2,128)(2,1)}, u32[]{:S(2)}, u32[]{:S(2)}) async-start(bf16[64,2,2048]{2,1,0:T(2,128)(2,1)} %get-tuple-element.14), calls=%async_computation.1 | async-start | bytes 1048576 | tf_op jit(solution)/shard_map/all_to_all | solution.py:474
  92.5 31.9 %copy-start.9 = (bf16[2048]{0:T(1024)(128)(2,1)S(1)}, bf16[2048]{0:T(1024)(128)(2,1)}, u32[]{:S(2)}) copy-start(bf16[2048]{0:T(1024)(128)(2,1)} %param.43) | copy-start | bytes 12292
  95.9 12.8 %copy-start.8 = (bf16[2048,128]{1,0:T(8,128)(2,1)S(1)}, bf16[2048,128]{1,0:T(8,128)(2,1)}, u32[]{:S(2)}) copy-start(bf16[2048,128]{1,0:T(8,128)(2,1)} %param.35) | copy-start | bytes 1572868
  95.9 23.4 %all-to-all-start.2 = ((bf16[64,2,2048]{2,1,0:T(2,128)(2,1)}), bf16[64,2,2048]{2,1,0:T(2,128)(2,1)S(1)}, u32[]{:S(2)}, u32[]{:S(2)}) async-start(bf16[64,2,2048]{2,1,0:T(2,128)(2,1)} %routed.1), calls=%async_computation.2 | async-start | bytes 1048576 | tf_op jit(solution)/shard_map/all_to_all | solution.py:493
  104.4 1.3 copy-start.1
  105.6 1.2 copy-start.2
  106.8 1.2 copy-start.3
  120.0 5.2 %collective-permute-start.7 = (f32[8,2048]{1,0:T(8,128)S(1)}, f32[8,2048]{1,0:T(8,128)S(1)}, u32[]{:S(2)}, u32[]{:S(2)}) collective-permute-start(f32[8,2048]{1,0:T(8,128)S(1)} %get-tuple-element.16), channel_id=1, source_target_pairs={{0,1},{1,0},{2,3},{3,2},{4,5},{5,4},{6,7},{7,6},{8,9},{9,8},{10,11... | collective-permute-start | bytes 196616 | tf_op jit(solution)/shard_map/ppermute | solution.py:63

commit v3 on v2

--- a/solution.py
+++ b/solution.py
@@ -8,7 +8,7 @@
 from jax.sharding import Mesh
 from jax.sharding import PartitionSpec as P
 
-SEQ_STEP = 2
+SEQ_STEP = 4
 EP = ("ep_0", "ep_1")
 GRP_EP_TP = ("grp", "ep_0", "ep_1", "tp")
 EP_TP = ("ep_0", "ep_1", "tp")
@@ -25,38 +25,63 @@
     return (row * 8 + col) * 2 + core
 
 
-PLACES = [
-    [
-        device_at(2 * block_row + i, 2 * block_col + j, core)
-        for block_row in range(4)
-        for block_col in range(4)
-    ]
-    for i in range(2)
-    for j in range(2)
+COLUMN_GROUPS = [[device_at(row, col, core) for col in range(8) for core in range(2)] for row in range(8)]
+BLOCKS = [
+    [device_at(row, 2 * pair + col, core) for row in range(8) for col in range(2)]
+    for pair in range(4)
     for core in range(2)
 ]
-
-
-def partners(flip_i, flip_j):
-    return [
-        (device_at(row, col, core), device_at(row ^ flip_i, col ^ flip_j, core))
-        for row in range(8)
-        for col in range(8)
-        for core in range(2)
-    ]
-
-
-def from_partner(array, flip):
-    return lax.ppermute(array, EP_TP, partners(flip // 2, flip % 2))
+HALVES = 2
+QUARTERS = 4
+
+
+def repeat_kernel(array_ref, out_ref):
+    run = out_ref.shape[-1]
+    count = array_ref.shape[-1] // run
+    for n in range(out_ref.shape[0]):
+        out_ref[n] = array_ref[:, n % count * run : (n % count + 1) * run]
+
+
+def in_parts(array, count, times):
+    rows, width = array.shape
+    return pl.pallas_call(
+        repeat_kernel,
+        in_specs=[pl.BlockSpec(memory_space=pltpu.VMEM)],
+        out_specs=pl.BlockSpec(memory_space=pltpu.VMEM),
+        out_shape=jax.ShapeDtypeStruct((count * times, rows, width // count), array.dtype),
+        compiler_params=pltpu.CompilerParams(vmem_limit_bytes=4 << 20),
+        name="parts",
+    )(array)
+
+
+def project_kernel(place_ref, heads_ref, own_slab_ref, other_slab_ref, out_ref):
+    core = place_ref[0]
+    heads = heads_ref[...].reshape(-1, heads_ref.shape[-1])
+    run = own_slab_ref.shape[-1]
+    first, second = heads[:, :run], heads[:, run:]
+    own = jnp.where(core == 0, first, second)
+    other = jnp.where(core == 0, second, first)
+    dims = (((1,), (1,)), ((), ()))
+    out = lax.dot_general(
+        own, own_slab_ref[...], dims, preferred_element_type=jnp.float32
+    ) + lax.dot_general(other, other_slab_ref[...], dims, preferred_element_type=jnp.float32)
+    out_ref[...] = out.astype(jnp.bfloat16).reshape(out_ref.shape)
+
+
+def projected(place, heads, own_slab, other_slab):
+    return pl.pallas_call(
+        project_kernel,
+        in_specs=[pl.BlockSpec(memory_space=pltpu.SMEM)]
+        + [pl.BlockSpec(memory_space=pltpu.VMEM)] * 3,
+        out_specs=pl.BlockSpec(memory_space=pltpu.VMEM),
+        out_shape=jax.ShapeDtypeStruct((*heads.shape[:2], own_slab.shape[0]), jnp.bfloat16),
+        compiler_params=pltpu.CompilerParams(vmem_limit_bytes=6 << 20),
+        name="projected",
+    )(place, heads, own_slab, other_slab)
 
 
 def exchanged(blocks, groups):
     return lax.all_to_all(blocks, EP_TP, 0, 0, axis_index_groups=groups, tiled=True)
-
-
-def sent_to_all(array, groups):
-    count = len(groups[0])
-    return exchanged(jnp.broadcast_to(array[None], (count, *array.shape)), groups)
 
 
 def from_other_core(array):
@@ -123,34 +148,52 @@
         key_new = turned(key_ref[...].astype(jnp.float32), cosine, sine)
         key_new_ref[...] = key_new.astype(jnp.bfloat16).astype(jnp.float32)[:, None, :]
 
-    for place in range(cache_ref.shape[0]):
-        seq = step * cache_ref.shape[0] + place
-        length = lengths_ref[seq]
-        query = query_ref[seq]
-        query_pe = query_pe_ref[seq]
-        latent_wide = latent_new_ref[seq]
-        score_new = (
-            jnp.sum(query.astype(jnp.float32) * latent_wide, axis=-1, keepdims=True)
-            + jnp.sum(query_pe.astype(jnp.float32) * key_new_ref[seq], axis=-1, keepdims=True)
-        ) * scale
-        cache = cache_ref[place]
-        scores = (
-            lax.dot_general(
-                query, cache, (((1,), (1,)), ((), ())), preferred_element_type=jnp.float32
+    places = range(cache_ref.shape[0])
+    seqs = [step * cache_ref.shape[0] + place for place in places]
+    rows = cache_ref.shape[0] * heads
+    query = query_ref[pl.ds(step * cache_ref.shape[0], cache_ref.shape[0])]
+    query_pe = query_pe_ref[pl.ds(step * cache_ref.shape[0], cache_ref.shape[0])]
+    latent_wide = latent_new_ref[pl.ds(step * cache_ref.shape[0], cache_ref.shape[0])]
+    key_wide = key_new_ref[pl.ds(step * cache_ref.shape[0], cache_ref.shape[0])]
+    score_new = (
+        jnp.sum(query.astype(jnp.float32) * latent_wide, axis=-1, keepdims=True)
+        + jnp.sum(query_pe.astype(jnp.float32) * key_wide, axis=-1, keepdims=True)
+    ).reshape(rows, 1) * scale
+    parts = [
+        lax.dot_general(
+            query[place], cache_ref[place], (((1,), (1,)), ((), ())),
+            preferred_element_type=jnp.float32,
+        )
+        + jnp.dot(query_pe[place], cache_rope_ref[place], preferred_element_type=jnp.float32)
+        for place in places
+    ]
+    position = lax.broadcasted_iota(jnp.int32, parts[0].shape, 1)
+    scores = jnp.concatenate(
+        [
+            jnp.where(position < lengths_ref[seq], part * scale, masked_score)
+            for seq, part in zip(seqs, parts)
+        ],
+        axis=0,
+    )
+    row_max = jnp.maximum(jnp.max(scores, axis=-1, keepdims=True), score_new)
+    weights = jnp.exp(scores - row_max)
+    weight_new = jnp.exp(score_new - row_max)
+    total = jnp.sum(weights, axis=-1, keepdims=True) + weight_new
+    rounded = weights.astype(jnp.bfloat16)
+    summed = jnp.concatenate(
+        [
+            jnp.dot(
+                rounded[place * heads : (place + 1) * heads],
+                cache_ref[place],
+                preferred_element_type=jnp.float32,
             )
-            + jnp.dot(query_pe, cache_rope_ref[place], preferred_element_type=jnp.float32)
-        ) * scale
-        position = lax.broadcasted_iota(jnp.int32, scores.shape, 1)
-        scores = jnp.where(position < length, scores, masked_score)
-        row_max = jnp.maximum(jnp.max(scores, axis=-1, keepdims=True), score_new)
-        weights = jnp.exp(scores - row_max)
-        weight_new = jnp.exp(score_new - row_max)
-        total = jnp.sum(weights, axis=-1, keepdims=True) + weight_new
-        summed = (
-            jnp.dot(weights.astype(jnp.bfloat16), cache, preferred_element_type=jnp.float32)
-            + weight_new.astype(jnp.bfloat16).astype(jnp.float32) * latent_wide
-        )
-        out_ref[place] = (summed / total).astype(jnp.bfloat16)
+            for place in places
+        ],
+        axis=0,
+    )
+    fresh = jnp.broadcast_to(latent_wide, query.shape).reshape(rows, latent)
+    summed = summed + weight_new.astype(jnp.bfloat16).astype(jnp.float32) * fresh
+    out_ref[...] = (summed / total).astype(jnp.bfloat16).reshape(out_ref.shape)
 
 
 def attended(query_nope, query_rope, new_latent, new_rope, cache_latent, cache_rope, lengths, absorb_key):
@@ -219,7 +262,8 @@
 
 def spread_kernel(
     place_ref,
-    pieces_ref,
+    own_pieces_ref,
+    other_pieces_ref,
     own_hidden_ref,
     other_hidden_ref,
     gain_mix_ref,
@@ -230,35 +274,27 @@
     mix_ref,
     taken_ref,
 ):
-    core, block_i, block_j = place_ref[0], place_ref[1], place_ref[2]
+    core = place_ref[0]
     half = own_hidden_ref.shape[0]
     rows = 2 * half
-    piece = pieces_ref.shape[-1]
-    run = piece // 4
-    chunks = []
-    for block_row in range(4):
-        for i in range(2):
-            runs = [
-                pieces_ref[
-                    c,
-                    (i ^ block_i) * 2 + (j ^ block_j),
-                    :,
-                    block_row * run : (block_row + 1) * run,
-                ]
-                for j in range(2)
-                for c in range(2)
-            ]
-            chunks.append(jnp.concatenate(runs, axis=-1))
-    joined = jnp.concatenate(chunks, axis=0)
-    source = lax.broadcasted_iota(jnp.int32, (piece, piece), 0)
-    target = lax.broadcasted_iota(jnp.int32, (piece, piece), 1)
-    k = run // 4
-    goes_to = (source % run) // k * run + source // run * k + source % k
-    order = jnp.where(goes_to == target, 1.0, 0.0).astype(jnp.bfloat16)
-    placed = jnp.dot(joined, order, preferred_element_type=jnp.float32)
+
+    def in_columns(pieces_ref):
+        parts = [
+            pieces_ref[HALVES * n].astype(jnp.float32) + pieces_ref[HALVES * n + 1].astype(jnp.float32)
+            for n in range(pieces_ref.shape[0] // HALVES)
+        ]
+        return jnp.concatenate(parts, axis=-1)
+
+    own_mixed = in_columns(own_pieces_ref)
+    other_mixed = in_columns(other_pieces_ref)
     mixed = jnp.concatenate(
-        [placed[n * rows : (n + 1) * rows] for n in range(len(chunks))], axis=-1
-    )
+        [
+            jnp.where(core == 0, own_mixed, other_mixed),
+            jnp.where(core == 0, other_mixed, own_mixed),
+        ],
+        axis=0,
+    )
+    mixed = mixed.astype(jnp.bfloat16).astype(jnp.float32)
     own_hidden = own_hidden_ref[...].astype(jnp.float32)
     other_hidden = other_hidden_ref[...].astype(jnp.float32)
     hidden = jnp.concatenate(
@@ -295,12 +331,12 @@
     outgoing_ref[...] = outgoing.reshape(outgoing_ref.shape)
 
 
-def spread(place, pieces, own_hidden, other_hidden, gain_mix, gain_in, routes, slots):
+def spread(place, own_pieces, other_pieces, own_hidden, other_hidden, gain_mix, gain_in, routes, slots):
     rows, width = 2 * own_hidden.shape[0], own_hidden.shape[1]
     return pl.pallas_call(
         spread_kernel,
         in_specs=[pl.BlockSpec(memory_space=pltpu.SMEM)]
-        + [pl.BlockSpec(memory_space=pltpu.VMEM)] * 6,
+        + [pl.BlockSpec(memory_space=pltpu.VMEM)] * 7,
         out_specs=[pl.BlockSpec(memory_space=pltpu.VMEM)] * 4,
         out_shape=[
             jax.ShapeDtypeStruct((slots // 2, 2, width), jnp.bfloat16),
@@ -310,7 +346,16 @@
         ],
         compiler_params=pltpu.CompilerParams(vmem_limit_bytes=8 << 20),
         name="spread",
-    )(place, pieces, own_hidden, other_hidden, gain_mix, gain_in, routes.T)
+    )(
+        place,
+        own_pieces,
+        other_pieces,
+        own_hidden,
+        other_hidden,
+        gain_mix,
+        gain_in,
+        routes.T,
+    )
 
 
 def experts_kernel(rows_ref, gate_ref, up_ref, down_ref, out_ref):
@@ -435,7 +480,10 @@
     seq_count, _ = hidden_in.shape
     core = lax.axis_index("tp")
     own_start = core * seq_count
-    slab = sent_to_all(out_proj.T, PLACES).reshape(-1, out_proj.shape[0])
+    place = core[None].astype(jnp.int32)
+    quarters = in_parts(out_proj.T, QUARTERS, len(COLUMN_GROUPS[0]) // QUARTERS)
+    slab = exchanged(quarters, COLUMN_GROUPS).reshape(-1, quarters.shape[-1])
+    other_slab = from_other_core(slab)
     other_hidden = from_other_core(hidden_in)
     heads_out = attention(
         query_nope,
@@ -448,20 +496,10 @@
         absorb_key,
         value_up,
     )
-    chip_heads = lax.all_gather(heads_out, "tp", axis=0, tiled=True)
-    block_heads = jnp.concatenate(
-        [chip_heads] + [from_partner(chip_heads, flip) for flip in range(1, 4)], axis=0
-    )
-    partial = lax.dot_general(
-        block_heads, slab, (((1,), (1,)), ((), ())), preferred_element_type=jnp.float32
-    ).astype(jnp.bfloat16)
-    chip_rows = partial.reshape(4, 2 * seq_count, -1)
-    pieces = jnp.stack(
-        [chip_rows[0]] + [from_partner(chip_rows[flip], flip) for flip in range(1, 4)]
-    )
-    pieces = lax.all_gather(pieces, "tp", axis=0)
-    place = jnp.stack([core, lax.axis_index("ep_0") % 2, lax.axis_index("ep_1") % 2])
-    place = place.astype(jnp.int32)
+    block_heads = exchanged(in_parts(heads_out, HALVES, len(BLOCKS[0]) // HALVES), BLOCKS)
+    partial = projected(place, block_heads, slab, other_slab)
+    pieces = exchanged(partial, BLOCKS)
+    other_pieces = from_other_core(pieces)
     experts_total = router.shape[1]
     group_rows, top_count = routes.shape
     ep_count = lax.axis_size(EP)
@@ -469,7 +507,15 @@
     slots = ep_count * capacity
     slot_expert = lax.iota(jnp.int32, slots) // capacity * 2 + core
     outgoing, ffn_in, own_mix, taken = spread(
-        place, pieces, hidden_in, other_hidden, gain_mix, gain_ffn_in, routes, slots
+        place,
+        pieces,
+        other_pieces,
+        hidden_in,
+        other_hidden,
+        gain_mix,
+        gain_ffn_in,
+        routes,
+        slots,
     )
     received = lax.all_to_all(
         outgoing, EP, split_axis=0, concat_axis=0, tiled=True

time: 127 us -> 125 us (0.984)
  waiting for transfers between devices: 40.5 us -> 44.8 us
  blocking collectives: 13 us -> 10.5 us
    all_to_all x1 -> x2, waiting for transfers between devices: 0.01 us -> 15.4 us  [exchanged(): lax.all_to_all(blocks, EP_TP, 0, 0, axis_index_groups=groups, tiled=True)]
    ppermute x6 -> x0, waiting for transfers between devices: 13.2 us -> none  [from_partner(): return lax.ppermute(array, EP_TP, partners(flip // 2, flip % 2))]
    all_gather x2 -> x0, blocking collectives: 13 us -> none  [the longest x1 6.98 us: local(): chip_heads = lax.all_gather(heads_out, 'tp', axis=0, tiled=True)]
    all_to_all x0 -> x1, blocking collectives: none -> 10.5 us  [exchanged(): lax.all_to_all(blocks, EP_TP, 0, 0, axis_index_groups=groups, tiled=True)]
    all_to_all x1 -> x2, starting transfers between devices: 19.2 us -> 27.7 us  [exchanged(): lax.all_to_all(blocks, EP_TP, 0, 0, axis_index_groups=groups, tiled=True)]
    ppermute x6 -> x0, starting transfers between devices: 5.4 us -> none  [from_partner(): return lax.ppermute(array, EP_TP, partners(flip // 2, flip % 2))]
    all_to_all x1, starting transfers between devices: 11.2 us -> 7.12 us  [local(): lax.all_to_all(outgoing, EP, split_axis=0, concat_axis=0, tiled=True)]
    broadcast_in_dim x1 -> x0, local copies, waits for them, and re-layouts: 2.03 us -> none  [sent_to_all(): jnp.broadcast_to(array[None], (count, *array.shape))]
  transfers between devices with their start and end apart: 11 -> 8, of which waited for: 7 -> 6; matrix products, arithmetic and copies ran while one was open for 2% -> 1% of each run, Pallas kernels for 6% -> 6%
where the time goes in v3:
time: 125 us; the launch traced here: 124 us
  starting transfers between devices  48.8 us (39%)
  waiting for transfers between devices  44.8 us (36%)
  Pallas kernels  12.9 us (10%)
  blocking collectives  10.5 us (8%)
  local copies, waits for them, and re-layouts  4.74 us (4%)
  matrix products  1.38 us (1%)
    all_to_all x2, starting transfers between devices, exchanged(): lax.all_to_all(blocks, EP_TP, 0, 0, axis_index_groups=groups, tiled=True)  27.7 us
    all_to_all x1, waiting for transfers between devices, local(): lax.all_to_all(outgoing, EP, split_axis=0, concat_axis=0, tiled=True)  16.8 us
    all_to_all x2, waiting for transfers between devices, exchanged(): lax.all_to_all(blocks, EP_TP, 0, 0, axis_index_groups=groups, tiled=True)  15.4 us
    all_to_all x1, blocking collectives, exchanged(): lax.all_to_all(blocks, EP_TP, 0, 0, axis_index_groups=groups, tiled=True)  10.5 us
    all_to_all x1, waiting for transfers between devices, local(): lax.all_to_all(outputs, EP, split_axis=0, concat_axis=0, tiled=True)  10.5 us
    all_to_all x1, starting transfers between devices, local(): lax.all_to_all(outputs, EP, split_axis=0, concat_axis=0, tiled=True)  8.13 us
    all_to_all x1, starting transfers between devices, local(): lax.all_to_all(outgoing, EP, split_axis=0, concat_axis=0, tiled=True)  7.12 us
    ppermute x4, starting transfers between devices, from_other_core(): return lax.ppermute(array, 'tp', [(0, 1), (1, 0)])  5.86 us
  transfers between devices with their start and end apart: 8, of which 6 were waited for; matrix products, arithmetic and copies ran while one was open for 1% of the time, Pallas kernels for 6%

profile of v3, /device:TPU:513, one launch (start us, length us, event | category | flops | bytes accessed | tf_op | source)
XLA Modules:
  0.0 124.5 jit_solution(8825574805132696688)
XLA Ops:
  0.0 0.0 copy-start
  0.0 0.0 copy-start.4
  0.0 0.9 copy-done.4
  0.9 0.7 parts.3
  1.6 23.7 %all-to-all-start.1 = ((bf16[16,16,512]{2,1,0:T(8,128)(2,1)}), bf16[16,16,512]{2,1,0:T(8,128)(2,1)S(1)}, u32[]{:S(2)}, u32[]{:S(2)}) async-start(bf16[16,16,512]{2,1,0:T(8,128)(2,1)} %parts.3), calls=%async_computation.1 | async-start | bytes 524288 | tf_op jit(solution)/shard_map/all_to_all | solution.py:84
  25.4 0.0 copy-start.6
  25.4 0.0 copy-start.5
  25.4 0.0 copy-start.7
  25.4 0.0 copy-start.8
  25.4 5.6 %attended.1 = bf16[8,16,256]{2,1,0:T(8,128)(2,1)} custom-call(s32[8]{0:T(128)} %lengths_ref.1, bf16[8,16,64]{2,1,0:T(8,128)(2,1)} %nope_ref.1, bf16[8,16,32]{2,1,0:T(8,128)(2,1)} %rope_ref.1, bf16[8,256]{1,0:T(8,128)(2,1)} %latent_ref.1, bf16[8,32]{1,0:T(8,128)(2,1)} %key_ref.1, bf16[1024,256]{1,0:T(8,128)(2,1)} %bitcast.32, ...), custom_call_target="tpu_custom_call" | custom-call | flops 268435456 | bytes 4718592 | tf_op jit(solution)/shard_map/attended/pallas_call | solution.py:207
  31.1 0.0 copy-done
  31.1 1.2 fusion.array_ref
  32.2 0.7 parts.2
  33.0 4.4 %all-to-all-done.1 = bf16[16,16,512]{2,1,0:T(8,128)(2,1)S(1)} async-done(((bf16[16,16,512]{2,1,0:T(8,128)(2,1)}), bf16[16,16,512]{2,1,0:T(8,128)(2,1)S(1)}, u32[]{:S(2)}, u32[]{:S(2)}) %all-to-all-start.1) | async-done | bytes 262176 | tf_op jit(solution)/shard_map/all_to_all | solution.py:84
  37.4 4.0 %all-to-all-start = ((bf16[16,8,1024]{2,1,0:T(8,128)(2,1)}), bf16[16,8,1024]{2,1,0:T(8,128)(2,1)S(1)}, u32[]{:S(2)}, u32[]{:S(2)}) async-start(bf16[16,8,1024]{2,1,0:T(8,128)(2,1)} %parts.2), calls=%async_computation | async-start | bytes 524288 | tf_op jit(solution)/shard_map/all_to_all | solution.py:84
  41.3 0.1 collective-permute-start
  41.5 11.0 %all-to-all-done.heads_ref = bf16[16,8,1024]{2,1,0:T(8,128)(2,1)S(1)} async-done(((bf16[16,8,1024]{2,1,0:T(8,128)(2,1)}), bf16[16,8,1024]{2,1,0:T(8,128)(2,1)S(1)}, u32[]{:S(2)}, u32[]{:S(2)}) %all-to-all-start) | async-done | bytes 262176 | tf_op jit(solution)/shard_map/all_to_all | solution.py:84
  52.5 0.0 collective-permute-done.other_slab_ref
  52.5 0.3 projected.1
  52.8 10.5 %all_to_all.25.own_pieces_ref = bf16[16,8,256]{2,1,0:T(8,128)(2,1)S(1)} all-to-all(bf16[16,8,256]{2,1,0:T(8,128)(2,1)S(1)} %projected.1), channel_id=1, replica_groups={{0,2,16,18,32,34,48,50,64,66,80,82,96,98,112,114},{1,3,17,19,33,35,49,5..., dimensions={0} | all-to-all | bytes 131072 | tf_op jit(solution)/shard_map/all_to_all | solution.py:84
  63.3 1.7 %collective-permute-start.1 = (bf16[16,8,256]{2,1,0:T(8,128)(2,1)S(1)}, bf16[16,8,256]{2,1,0:T(8,128)(2,1)S(1)}, u32[]{:S(2)}, u32[]{:S(2)}) collective-permute-start(bf16[16,8,256]{2,1,0:T(8,128)(2,1)S(1)} %all_to_all.25.own_pieces_ref), channel_id=1, source_target_pairs={{0,1},{1,0},{2,3},{3,2},{4,5},{5,4},{6,7},{7,6},{8,9},{9,8},{10,11... | collective-permute-start | bytes 196616 | tf_op jit(solution)/shard_map/ppermute | solution.py:88
  65.1 0.0 copy-done.6
  65.1 0.0 collective-permute-start.2
  65.1 1.2 collective-permute-done.2.other_hidden_ref
  66.3 0.0 collective-permute-done.1.other_pieces_ref
  66.3 0.0 copy-done.5
  66.3 0.0 copy-done.7
  66.3 0.0 copy-done.8
  66.3 1.3 %spread.1 = (bf16[64,2,2048]{2,1,0:T(2,128)(2,1)}, bf16[16,2048]{1,0:T(8,128)(2,1)S(1)}, bf16[8,2048]{1,0:T(8,128)(2,1)S(1)}, bf16[128,16]{1,0:T(8,128)(2,1)S(1)}) custom-call(s32[1]{0:T(128)} %bitcast.place_ref, bf16[16,8,256]{2,1,0:T(8,128)(2,1)S(1)} %all_to_all.25.own_pieces_ref, bf16[16,8,256]{2,1,0:T(8,128)(2,1)S(1)} %collective-permute-done.1.other_pieces_ref, ...), custom_call_target="tpu_custom_call" | custom-call | tf_op jit(solution)/shard_map/spread/pallas_call | solution.py:336
  67.6 7.1 %all-to-all-start.3 = ((bf16[64,2,2048]{2,1,0:T(2,128)(2,1)}), bf16[64,2,2048]{2,1,0:T(2,128)(2,1)}, u32[]{:S(2)}, u32[]{:S(2)}) async-start(bf16[64,2,2048]{2,1,0:T(2,128)(2,1)} %get-tuple-element.14), calls=%async_computation.3 | async-start | bytes 1048576 | tf_op jit(solution)/shard_map/all_to_all | solution.py:520
  74.8 16.8 %all-to-all-done.3.rows_hbm = bf16[64,2,2048]{2,1,0:T(2,128)(2,1)} async-done(((bf16[64,2,2048]{2,1,0:T(2,128)(2,1)}), bf16[64,2,2048]{2,1,0:T(2,128)(2,1)}, u32[]{:S(2)}, u32[]{:S(2)}) %all-to-all-start.3) | async-done | bytes 524320 | tf_op jit(solution)/shard_map/all_to_all | solution.py:520
  91.6 0.0 copy-start.10
  91.6 3.4 %routed.1 = bf16[64,2,2048]{2,1,0:T(2,128)(2,1)} custom-call(bf16[64,2,2048]{2,1,0:T(2,128)(2,1)} %all-to-all-done.3.rows_hbm, bf16[2048,256]{1,0:T(8,128)(2,1)} %bitcast.29, bf16[2048,256]{1,0:T(8,128)(2,1)} %bitcast.30, bf16[256,2048]{1,0:T(8,128)(2,1)} %bitcast.31), custom_call_target="tpu_custom_call" | custom-call | tf_op jit(solution)/shard_map/routed/pallas_call | solution.py:444
  95.0 0.0 copy-start.9
  95.0 8.1 %all-to-all-start.4 = ((bf16[64,2,2048]{2,1,0:T(2,128)(2,1)}), bf16[64,2,2048]{2,1,0:T(2,128)(2,1)S(1)}, u32[]{:S(2)}, u32[]{:S(2)}) async-start(bf16[64,2,2048]{2,1,0:T(2,128)(2,1)} %routed.1), calls=%async_computation.4 | async-start | bytes 1048576 | tf_op jit(solution)/shard_map/all_to_all | solution.py:539
  103.1 0.1 copy.29
  103.2 0.0 copy-start.1
  103.2 1.2 %copy-done.1 = bf16[2048,256]{1,0:T(8,128)(2,1)S(1)} copy-done((bf16[2048,256]{1,0:T(8,128)(2,1)S(1)}, bf16[2048,256]{1,0:T(8,128)(2,1)}, u32[]{:S(2)}) %copy-start.1) | copy-done | bytes 1048600
  104.5 0.0 copy-start.2
  104.5 1.2 copy-done.2
  105.7 0.0 copy-start.3
  105.7 1.2 copy-done.3
  106.9 0.6 shard_map.208.shared_ref
  107.5 0.0 copy-done.9
  107.5 0.2 fusion.3
  107.7 0.2 select_reduce_fusion
  108.0 0.1 select_reduce_fusion.2
  108.1 10.5 %all-to-all-done.4.returned_ref = bf16[64,2,2048]{2,1,0:T(2,128)(2,1)S(1)} async-done(((bf16[64,2,2048]{2,1,0:T(2,128)(2,1)}), bf16[64,2,2048]{2,1,0:T(2,128)(2,1)S(1)}, u32[]{:S(2)}, u32[]{:S(2)}) %all-to-all-start.4) | async-done | bytes 524320 | tf_op jit(solution)/shard_map/all_to_all | solution.py:539
  118.6 0.2 gathered.1
  118.8 4.0 %collective-permute-start.3 = (f32[8,2048]{1,0:T(8,128)S(1)}, f32[8,2048]{1,0:T(8,128)S(1)}, u32[]{:S(2)}, u32[]{:S(2)}) collective-permute-start(f32[8,2048]{1,0:T(8,128)S(1)} %get-tuple-element.16), channel_id=1, source_target_pairs={{0,1},{1,0},{2,3},{3,2},{4,5},{5,4},{6,7},{7,6},{8,9},{9,8},{10,11... | collective-permute-start | bytes 196616 | tf_op jit(solution)/shard_map/ppermute | solution.py:88
  122.7 0.0 copy-done.10
  122.7 0.9 collective-permute-done.3
  123.6 0.1 multiply_reduce_fusion
  123.8 0.7 add_convert_fusion
  (7 shorter events, 0.0 us)
Async XLA Ops:
  0.0 31.1 %copy-start = (bf16[256,16,128]{2,1,0:T(8,128)(2,1)S(1)}, bf16[256,16,128]{2,1,0:T(8,128)(2,1)}, u32[]{:S(2)}) copy-start(bf16[256,16,128]{2,1,0:T(8,128)(2,1)} %param.31) | copy-start | bytes 3145732
  0.0 0.9 copy-start.4
  1.6 35.7 %all-to-all-start.1 = ((bf16[16,16,512]{2,1,0:T(8,128)(2,1)}), bf16[16,16,512]{2,1,0:T(8,128)(2,1)S(1)}, u32[]{:S(2)}, u32[]{:S(2)}) async-start(bf16[16,16,512]{2,1,0:T(8,128)(2,1)} %parts.3), calls=%async_computation.1 | async-start | bytes 524288 | tf_op jit(solution)/shard_map/all_to_all | solution.py:84
  25.4 39.7 %copy-start.6 = (bf16[8,2048]{1,0:T(8,128)(2,1)S(1)}, bf16[8,2048]{1,0:T(8,128)(2,1)}, u32[]{:S(2)}) copy-start(bf16[8,2048]{1,0:T(8,128)(2,1)} %own_hidden_ref.1) | copy-start | bytes 98308
  25.4 40.9 %copy-start.5 = (s32[16,6]{0,1:T(8,128)S(1)}, s32[16,6]{0,1:T(8,128)}, u32[]{:S(2)}) copy-start(s32[16,6]{0,1:T(8,128)} %param.36) | copy-start | bytes 1156
  25.4 40.9 %copy-start.7 = (bf16[2048]{0:T(1024)(128)(2,1)S(1)}, bf16[2048]{0:T(1024)(128)(2,1)}, u32[]{:S(2)}) copy-start(bf16[2048]{0:T(1024)(128)(2,1)} %gain_mix_ref.1) | copy-start | bytes 12292
  25.4 40.9 %copy-start.8 = (bf16[2048]{0:T(1024)(128)(2,1)S(1)}, bf16[2048]{0:T(1024)(128)(2,1)}, u32[]{:S(2)}) copy-start(bf16[2048]{0:T(1024)(128)(2,1)} %gain_in_ref.1) | copy-start | bytes 12292
  37.4 15.2 %all-to-all-start = ((bf16[16,8,1024]{2,1,0:T(8,128)(2,1)}), bf16[16,8,1024]{2,1,0:T(8,128)(2,1)S(1)}, u32[]{:S(2)}, u32[]{:S(2)}) async-start(bf16[16,8,1024]{2,1,0:T(8,128)(2,1)} %parts.2), calls=%async_computation | async-start | bytes 524288 | tf_op jit(solution)/shard_map/all_to_all | solution.py:84
  41.3 11.2 %collective-permute-start = (bf16[256,512]{1,0:T(8,128)(2,1)S(1)}, bf16[256,512]{1,0:T(8,128)(2,1)S(1)}, u32[]{:S(2)}, u32[]{:S(2)}) collective-permute-start(bf16[256,512]{1,0:T(8,128)(2,1)S(1)} %bitcast.25), channel_id=1, source_target_pairs={{0,1},{1,0},{2,3},{3,2},{4,5},{5,4},{6,7},{7,6},{8,9},{9,8},{10,11... | collective-permute-start | bytes 786440 | tf_op jit(solution)/shard_map/ppermute | solution.py:88
  63.3 3.0 %collective-permute-start.1 = (bf16[16,8,256]{2,1,0:T(8,128)(2,1)S(1)}, bf16[16,8,256]{2,1,0:T(8,128)(2,1)S(1)}, u32[]{:S(2)}, u32[]{:S(2)}) collective-permute-start(bf16[16,8,256]{2,1,0:T(8,128)(2,1)S(1)} %all_to_all.25.own_pieces_ref), channel_id=1, source_target_pairs={{0,1},{1,0},{2,3},{3,2},{4,5},{5,4},{6,7},{7,6},{8,9},{9,8},{10,11... | collective-permute-start | bytes 196616 | tf_op jit(solution)/shard_map/ppermute | solution.py:88
  65.1 1.2 collective-permute-start.2
  67.6 24.0 %all-to-all-start.3 = ((bf16[64,2,2048]{2,1,0:T(2,128)(2,1)}), bf16[64,2,2048]{2,1,0:T(2,128)(2,1)}, u32[]{:S(2)}, u32[]{:S(2)}) async-start(bf16[64,2,2048]{2,1,0:T(2,128)(2,1)} %get-tuple-element.14), calls=%async_computation.3 | async-start | bytes 1048576 | tf_op jit(solution)/shard_map/all_to_all | solution.py:520
  91.6 31.2 %copy-start.10 = (bf16[2048]{0:T(1024)(128)(2,1)S(1)}, bf16[2048]{0:T(1024)(128)(2,1)}, u32[]{:S(2)}) copy-start(bf16[2048]{0:T(1024)(128)(2,1)} %param.43) | copy-start | bytes 12292
  95.0 12.5 %copy-start.9 = (bf16[2048,128]{1,0:T(8,128)(2,1)S(1)}, bf16[2048,128]{1,0:T(8,128)(2,1)}, u32[]{:S(2)}) copy-start(bf16[2048,128]{1,0:T(8,128)(2,1)} %param.35) | copy-start | bytes 1572868
  95.0 23.6 %all-to-all-start.4 = ((bf16[64,2,2048]{2,1,0:T(2,128)(2,1)}), bf16[64,2,2048]{2,1,0:T(2,128)(2,1)S(1)}, u32[]{:S(2)}, u32[]{:S(2)}) async-start(bf16[64,2,2048]{2,1,0:T(2,128)(2,1)} %routed.1), calls=%async_computation.4 | async-start | bytes 1048576 | tf_op jit(solution)/shard_map/all_to_all | solution.py:539
  103.2 1.3 %copy-start.1 = (bf16[2048,256]{1,0:T(8,128)(2,1)S(1)}, bf16[2048,256]{1,0:T(8,128)(2,1)}, u32[]{:S(2)}) copy-start(bf16[2048,256]{1,0:T(8,128)(2,1)} %gate_ref.1) | copy-start | bytes 3145732
  104.5 1.2 copy-start.2
  105.7 1.2 copy-start.3
  118.8 4.9 %collective-permute-start.3 = (f32[8,2048]{1,0:T(8,128)S(1)}, f32[8,2048]{1,0:T(8,128)S(1)}, u32[]{:S(2)}, u32[]{:S(2)}) collective-permute-start(f32[8,2048]{1,0:T(8,128)S(1)} %get-tuple-element.16), channel_id=1, source_target_pairs={{0,1},{1,0},{2,3},{3,2},{4,5},{5,4},{6,7},{7,6},{8,9},{9,8},{10,11... | collective-permute-start | bytes 196616 | tf_op jit(solution)/shard_map/ppermute | solution.py:88
